TPU v7x, 32 devices: a whole 2x2x4 slice. The times are simulated.
32 devices in a mesh: gr: 2 (over y), sp: 4 (over z), tp: 4 (over x, core).
Axes of the slice: x: 2, y: 2, z: 4, core: 2. Of those that a mesh axis runs over, the one named last changes fastest.
Arguments:
- tokens: bfloat16 [4, 1024, 4096], P('gr', ('sp', 'tp')), parts along dimension 0, may hold values from -6 to 6
- norm_gain: bfloat16 [4096], replicated, may hold values from 0.099609375 to 1.8984375
- key_weight: bfloat16 [4096, 1024], P(None, 'tp'), may hold values from -0.09375 to 0.09375
- value_weight: bfloat16 [4096, 1024], P(None, 'tp'), may hold values from -0.09375 to 0.09375
- cum_gates: float32 [4, 1024, 16], P('gr', 'sp', 'tp'), parts along dimension 0, may hold values from -173 to 0, as said below
- new_query: bfloat16 [4, 1024], P('gr', 'tp'), parts along dimension 0, may hold values from -240 to 240
- new_key: bfloat16 [4, 1024], P('gr', 'tp'), parts along dimension 0, may hold values from -6 to 6
- new_value: bfloat16 [4, 1024], P('gr', 'tp'), parts along dimension 0, may hold values from -6 to 6
- new_gate: float32 [4, 16], P('gr', 'tp'), parts along dimension 0, may hold values from -5 to -1.5
Outputs:
- key_cache: bfloat16 [4, 1024, 1024], P('gr', 'sp', 'tp'), parts along dimension 0
- value_cache: bfloat16 [4, 1024, 1024], P('gr', 'sp', 'tp'), parts along dimension 0
- readout: bfloat16 [4, 1024], P('gr', 'tp'), parts along dimension 0
There are 2 independent parts, one for each index of `gr`. A program takes and returns all parts, laid end to end along the dimension named above; an argument that names none is the same for every part. Nothing has to cross between parts.
Inputs may be any that keep to these rules, and one draw needn't show every extreme that they name: `cum_gates`: along positions, for each prompt and head, the values never rise.
All inputs are finite; a program needn't handle non-finite values.
Results may differ from a plain program's by a relative error of at most 0.005.
The roundings to bfloat16 on the way count: a program that leaves them out, or rounds other values in their place, can miss the bound.
Values may be sent and summed in bfloat16 or wider, within the bound.
A program may use at most 64 MiB of HBM per device.

v0:
```python
import functools

import jax
import jax.numpy as jnp
from jax import lax
from jax.experimental import pallas as pl
from jax.experimental.pallas import tpu as pltpu
from jax.sharding import PartitionSpec as P

HD = 64
CORES = 2

epsilon = 1e-06
masked_score = -1e30
MESH = pl.DeviceIdType.MESH


def kernel(
    dims,
    tok_hbm, gain_hbm, wk_hbm, wv_hbm, gates_hbm, q_hbm, nk_hbm, nv_hbm, ng_hbm,
    kbuf, vbuf, ro_ref,
    tok, inv, nb, acc, wbuf, gain_v, gain_row, gates_v, q_v, nk_v, nv_v, ng_v, stats,
    loc_sem, w_sem, small_sem, hop_sem,
    sx_sem, rx_sem, sp_sem, rp_sem, sr_sem, rr_sem, sz_sem, rz_sem,
):
    S, L, R, T, Z = dims
    X = T // CORES
    rows_each, D = tok.shape
    NC, KC = nb.shape[1], nb.shape[3]
    blocks = rows_each // R
    C = kbuf.shape[2]
    H = C // HD
    BL = T * L
    tp = lax.axis_index("tp")
    z = lax.axis_index("sp")
    x, c = tp // CORES, tp % CORES
    partner = x * CORES + (CORES - 1 - c)

    def rows(j):
        return pl.ds(j * R, R)

    loads = [pltpu.make_async_copy(tok_hbm.at[rows(j)], tok.at[rows(j)], loc_sem.at[j]) for j in range(blocks)]
    for copy in loads:
        copy.start()
    w_copies = [
        pltpu.make_async_copy(wk_hbm, wbuf.at[:, pl.ds(0, C)], w_sem.at[0]),
        pltpu.make_async_copy(wv_hbm, wbuf.at[:, pl.ds(C, C)], w_sem.at[1]),
    ]
    small = [
        pltpu.make_async_copy(src, dst, small_sem.at[i])
        for i, (src, dst) in enumerate(
            [(gain_hbm, gain_v), (gates_hbm, gates_v), (q_hbm, q_v), (nk_hbm, nk_v), (nv_hbm, nv_v), (ng_hbm, ng_v)]
        )
    ]
    for copy in small:
        copy.start()
    barrier = pltpu.get_barrier_semaphore()
    pl.semaphore_signal(barrier, inc=1, device_id={"tp": partner}, device_id_type=MESH)
    for d in range(1, X):
        pl.semaphore_signal(
            barrier, inc=1, device_id={"tp": ((x + d) % X) * CORES + c}, device_id_type=MESH
        )
    sides = (z > 0).astype(jnp.int32) + (z < Z - 1).astype(jnp.int32)

    def greet_sides(sem):
        @pl.when(z > 0)
        def _():
            pl.semaphore_signal(sem, inc=1, device_id={"sp": z - 1}, device_id_type=MESH)

        @pl.when(z < Z - 1)
        def _():
            pl.semaphore_signal(sem, inc=1, device_id={"sp": z + 1}, device_id_type=MESH)

    greet_sides(barrier)

    small[0].wait()
    g = gain_v[...].astype(jnp.float32)
    lanes = g.shape[1]
    for i in range(g.shape[0]):
        gain_row[:, pl.ds(i * lanes, lanes)] = g[i : i + 1, :]
    for j in range(blocks):
        loads[j].wait()
        if j == blocks - 1:
            for copy in w_copies:
                copy.start()
        v = tok[rows(j), :].astype(jnp.float32)
        r = lax.rsqrt(jnp.mean(v * v, axis=-1, keepdims=True) + epsilon)
        inv[rows(j), :] = jnp.broadcast_to(r, (R, KC))

    def x_copy(d, j):
        return pltpu.make_async_remote_copy(
            nb.at[tp, j], nb.at[tp, j], sx_sem.at[d - 1, j], rx_sem.at[d - 1, j],
            device_id={"tp": ((x + d) % X) * CORES + c}, device_id_type=MESH,
        )

    def x_source(d, core):
        return ((x + X - d) % X) * CORES + core

    def relay_copy(d, j):
        t = x_source(d, c)
        return pltpu.make_async_remote_copy(
            nb.at[t, j], nb.at[t, j], sr_sem.at[d - 1, j], rr_sem.at[d - 1, j],
            device_id={"tp": partner}, device_id_type=MESH,
        )

    def arrival(t, j, sem):
        return pltpu.make_async_remote_copy(
            nb.at[t, j], nb.at[t, j], sem, sem,
            device_id={"tp": partner}, device_id_type=MESH,
        )

    def norm(k):
        part = pl.ds(k * KC, KC)
        v = tok[:, part].astype(jnp.float32)
        nb[tp, k] = (v * inv[...] * gain_row[:, part]).astype(jnp.bfloat16)

    norm(0)
    norm(1)
    pl.semaphore_wait(barrier, 1 + (X - 1) + sides)
    for k in range(NC):
        for d in range(1, X):
            x_copy(d, k).start()
        if k + 2 < NC:
            norm(k + 2)
    own_to_partner = pltpu.make_async_remote_copy(
        nb.at[tp], nb.at[tp], sp_sem, rp_sem, device_id={"tp": partner}, device_id_type=MESH
    )
    own_to_partner.start()
    if Z > 2:
        greet_sides(hop_sem.at[0])

    for copy in small[1:]:
        copy.wait()
    acc[...] = jnp.zeros_like(acc)

    def project(group, k, first, second):
        part = pl.ds(pl.multiple_of(k * KC, KC), KC)
        both = jnp.concatenate([nb[first, k], nb[second, k]], axis=0)
        acc[group] += jnp.dot(both, wbuf[part, :], preferred_element_type=jnp.float32)

    def keep(group, first, second):
        for i, t in enumerate((first, second)):
            for s in range(S):
                y = acc[group, pl.ds(i * rows_each + s * L, L), :].astype(jnp.bfloat16)
                at = pl.ds(pl.multiple_of(t * L, L), L)
                kbuf[s, at, :] = y[:, :C]
                vbuf[s, at, :] = y[:, C:]

    for copy in w_copies:
        copy.wait()
    pltpu.make_async_remote_copy(
        nb.at[partner], nb.at[partner], sp_sem, rp_sem, device_id={"tp": partner}, device_id_type=MESH
    ).wait_recv()

    def near(k, carry):
        project(0, k, tp, partner)
        return carry

    lax.fori_loop(0, NC, near, 0)
    keep(0, tp, partner)
    for r in range(1, Z - 2):
        pl.semaphore_wait(hop_sem.at[r - 1], sides)
        greet_sides(hop_sem.at[r])

    def arrive(k):
        for d in range(1, X):
            arrival(x_source(d, c), k, rx_sem.at[d - 1, k]).wait_recv()
            relay_copy(d, k).start()

    def use(k):
        for d in range(1, X):
            first, second = x_source(d, c), x_source(d, CORES - 1 - c)
            arrival(second, k, rr_sem.at[d - 1, k]).wait_recv()
            project(d, k, first, second)

    def far(k, carry):
        arrive(k)
        use(k - 1)
        return carry

    arrive(0)
    lax.fori_loop(1, NC, far, 0)
    use(NC - 1)
    for d in range(1, X):
        keep(d, x_source(d, c), x_source(d, CORES - 1 - c))

    scale = HD ** (-0.5)
    head_of_lane = lax.broadcasted_iota(jnp.int32, (H, C), 1) // HD
    own_head = head_of_lane == lax.broadcasted_iota(jnp.int32, (H, C), 0)
    eye = lax.broadcasted_iota(jnp.int32, (H, H), 0) == lax.broadcasted_iota(jnp.int32, (H, H), 1)
    last_block = z == Z - 1

    def as_row(column):
        return jnp.sum(jnp.where(own_head, column, 0.0), axis=0, keepdims=True)

    for s in range(S):
        qd = jnp.where(own_head, q_v[s : s + 1, :].astype(jnp.float32), 0.0)
        fresh = jnp.sum(qd * nk_v[s : s + 1, :].astype(jnp.float32), axis=1, keepdims=True) * scale
        gates = gates_v[s]
        own_gate = jnp.sum(jnp.where(eye, ng_v[s : s + 1, :], 0.0), axis=1, keepdims=True)
        fresh = jnp.where(last_block, fresh - (gates[:, BL - 1 : BL] + own_gate), masked_score)
        scores = lax.dot_general(
            qd.astype(jnp.bfloat16), kbuf[s], (((1,), (1,)), ((), ())), preferred_element_type=jnp.float32
        )
        scores = scores * scale - gates
        top = jnp.maximum(jnp.max(scores, axis=1, keepdims=True), fresh)
        weights = jnp.exp(scores - top)
        fresh_weight = jnp.exp(fresh - top)
        total = jnp.sum(weights, axis=1, keepdims=True) + fresh_weight
        high = weights.astype(jnp.bfloat16)
        low = (weights - high.astype(jnp.float32)).astype(jnp.bfloat16)
        values = vbuf[s]
        weighted = jnp.dot(high, values, preferred_element_type=jnp.float32)
        weighted = weighted + jnp.dot(low, values, preferred_element_type=jnp.float32)
        weighted = weighted + fresh_weight * nv_v[s : s + 1, :].astype(jnp.float32)
        stats[z, 0, s : s + 1, :] = as_row(top)
        stats[z, 1, s : s + 1, :] = as_row(total)
        stats[z, 2, s : s + 1, :] = as_row(weighted)

    def z_copy(d):
        return pltpu.make_async_remote_copy(
            stats.at[z], stats.at[z], sz_sem.at[d - 1], rz_sem.at[d - 1],
            device_id={"sp": (z + d) % Z}, device_id_type=MESH,
        )

    if Z > 2:
        pl.semaphore_wait(hop_sem.at[Z - 3], sides)
    for d in range(1, Z):
        z_copy(d).start()
    for d in range(1, X):
        for j in range(NC):
            x_copy(d, j).wait_send()
            relay_copy(d, j).wait_send()
    own_to_partner.wait_send()
    for d in range(1, Z):
        source = (z + Z - d) % Z
        pltpu.make_async_remote_copy(
            stats.at[source], stats.at[source], sz_sem.at[d - 1], rz_sem.at[d - 1],
            device_id={"sp": source}, device_id_type=MESH,
        ).wait_recv()
    everything = stats[...]
    tops, totals, sums = everything[:, 0], everything[:, 1], everything[:, 2]
    factor = jnp.exp(tops - jnp.max(tops, axis=0, keepdims=True))
    ro_ref[...] = (jnp.sum(sums * factor, axis=0) / jnp.sum(totals * factor, axis=0)).astype(ro_ref.dtype)
    for d in range(1, Z):
        z_copy(d).wait_send()


def write_out(*refs):
    sems = refs[-1]
    count = (len(refs) - 1) // 2
    copies = [pltpu.make_async_copy(refs[i], refs[count + i], sems.at[i]) for i in range(count)]
    for copy in copies:
        copy.start()
    for copy in copies:
        copy.wait()


def body(
    tokens, norm_gain, key_weight, value_weight, cum_gates, new_query, new_key, new_value, new_gate
):
    S, L, D = tokens.shape
    C = key_weight.shape[1]
    H = C // HD
    T = lax.axis_size("tp")
    Z = lax.axis_size("sp")
    X = T // CORES
    BL = T * L
    R = 16 if L % 16 == 0 else L
    KC = 256 if D % 256 == 0 else D // 2
    NC = D // KC
    bf, f32 = jnp.bfloat16, jnp.float32
    hbm = pl.BlockSpec(memory_space=pltpu.HBM)
    dma = pltpu.SemaphoreType.DMA
    far = max(X - 1, 1)
    vmem = pl.BlockSpec(memory_space=pltpu.VMEM)
    results = pl.pallas_call(
        functools.partial(kernel, (S, L, R, T, Z)),
        out_shape=(
            pltpu.VMEM((S, BL, C), bf),
            pltpu.VMEM((S, BL, C), bf),
            pltpu.VMEM((S, C), bf),
        ),
        in_specs=[hbm] * 9,
        out_specs=(vmem, vmem, vmem),
        scratch_shapes=[
            pltpu.VMEM((S * L, D), bf),
            pltpu.VMEM((S * L, KC), f32),
            pltpu.VMEM((T, NC, S * L, KC), bf),
            pltpu.VMEM((X, 2 * S * L, 2 * C), f32),
            pltpu.VMEM((D, 2 * C), bf),
            pltpu.VMEM((D // 128, 128), bf),
            pltpu.VMEM((1, D), f32),
            pltpu.VMEM((S, H, BL), f32),
            pltpu.VMEM((S, C), bf),
            pltpu.VMEM((S, C), bf),
            pltpu.VMEM((S, C), bf),
            pltpu.VMEM((S, H), f32),
            pltpu.VMEM((Z, 3, S, C), f32),
            dma((S * L // R,)), dma((2,)), dma((6,)), pltpu.SemaphoreType.REGULAR((max(Z - 2, 1),)),
            dma((far, NC)), dma((far, NC)), dma, dma,
            dma((far, NC)), dma((far, NC)), dma((max(Z - 1, 1),)), dma((max(Z - 1, 1),)),
        ],
        compiler_params=pltpu.CompilerParams(
            collective_id=0, has_side_effects=True, vmem_limit_bytes=56 * 1024 * 1024
        ),
    )(
        tokens.reshape(S * L, D),
        norm_gain.reshape(D // 128, 128),
        key_weight,
        value_weight,
        jnp.transpose(cum_gates, (0, 2, 1)),
        new_query,
        new_key,
        new_value,
        new_gate,
    )
    return pl.pallas_call(
        write_out,
        out_shape=tuple(jax.ShapeDtypeStruct(r.shape, r.dtype) for r in results),
        in_specs=[vmem] * 3,
        out_specs=(hbm, hbm, hbm),
        scratch_shapes=[dma((3,))],
    )(*(pltpu.with_memory_space_constraint(r, pltpu.VMEM) for r in results))


def solution(mesh):
    in_specs = (
        P("gr", ("sp", "tp"), None),
        P(),
        P(None, "tp"),
        P(None, "tp"),
        P("gr", "sp", "tp"),
        P("gr", "tp"),
        P("gr", "tp"),
        P("gr", "tp"),
        P("gr", "tp"),
    )
    out_specs = (P("gr", "sp", "tp"), P("gr", "sp", "tp"), P("gr", "tp"))
    return jax.shard_map(body, mesh=mesh, in_specs=in_specs, out_specs=out_specs, check_vma=False)
```

profile of v0, /device:TPU:0, one launch (start us, length us, event | category | flops | bytes accessed | tf_op | source)
XLA Modules:
  0.0 36.9 jit_solution(4195655821460762547)
XLA Ops:
  0.6 35.4 %shard_map.112 = (bf16[2,256,256]{2,1,0:T(8,128)(2,1)S(1)}, bf16[2,256,256]{2,1,0:T(8,128)(2,1)S(1)}, bf16[2,256]{1,0:T(2,128)(2,1)S(1)}) custom-call(bf16[128,4096]{1,0:T(8,128)(2,1)} %bitcast.3, bf16[32,128]{1,0:T(8,128)(2,1)} %bitcast.4, bf16[4096,256]{1,0:T(8,128)(2,1)} %wk_hbm.1, bf16[4096,256]{1,0:T(8,128)(2,1)} %wv_hbm.1, f32[2,4,256]{2,1,0:T(4,128)} %bitcast.5, ...), custom_call_target="tpu_custom_call" | custom-call | tf_op jit(solution)/shard_map/pallas_call | solution.py:277
  36.1 0.8 %shard_map.113 = (bf16[2,256,256]{2,1,0:T(8,128)(2,1)}, bf16[2,256,256]{2,1,0:T(8,128)(2,1)}, bf16[2,256]{1,0:T(2,128)(2,1)}) custom-call(bf16[2,256,256]{2,1,0:T(8,128)(2,1)S(1)} %get-tuple-element.6.refs_0_, bf16[2,256,256]{2,1,0:T(8,128)(2,1)S(1)} %get-tuple-element.7.refs_1_, bf16[2,256]{1,0:T(2,128)(2,1)S(1)} %get-tuple-element.8.refs_2_), custom_call_target="tpu_custom_call" | custom-call | tf_op jit(solution)/shard_map/pallas_call | solution.py:318
where the time goes:
time: 37 us; the launch traced here: 36.9 us
  Pallas kernels  36.3 us (98%)
  between operations  0.64 us (2%)
    pallas_call x1, Pallas kernels, body(): pl.pallas_call(functools.partial(kernel, (S, L, R, T, Z)), out_shape=(plt...  35.4 us
    pallas_call x1, Pallas kernels, body(): pl.pallas_call(write_out, out_shape=tuple((jax.ShapeDtypeStruct(r.shape,...  0.82 us

commit v1 on v0

v1 whole, which is shorter than its diff:
```python
import functools

import jax
import jax.numpy as jnp
from jax import lax
from jax.experimental import pallas as pl
from jax.experimental.pallas import tpu as pltpu
from jax.sharding import PartitionSpec as P

HD = 64
CORES = 2
RAW = 1

epsilon = 1e-06
masked_score = -1e30
MESH = pl.DeviceIdType.MESH


def kernel(
    dims,
    tok_hbm, gain_hbm, wk_hbm, wv_hbm, gates_hbm, q_hbm, nk_hbm, nv_hbm, ng_hbm,
    kbuf, vbuf, ro_ref,
    tok, raw, inv, nb, rx, acc, wbuf, ybuf, gain_v, gain_row, gates_v, q_v, nk_v, nv_v, ng_v,
    inv_tx, inv_rx, qblock, gate_rep, stats_tx, stats_rx,
    loc_sem, raw_sem, w_sem, small_sem, hop_sem, ready_sem,
    sx_sem, rx_sem, si_sem, ri_sem, sw_sem, rw_sem, sy_sem, ry_sem, sz_sem, rz_sem,
):
    S, L, R, T, Z = dims
    X = T // CORES
    f32, bf = jnp.float32, jnp.bfloat16
    rows_each, D = tok.shape
    NC, KC = nb.shape[0], nb.shape[2]
    blocks = rows_each // R
    C = kbuf.shape[2]
    H = C // HD
    BL = T * L
    tp = lax.axis_index("tp")
    z = lax.axis_index("sp")
    x, c = tp // CORES, tp % CORES
    partner = x * CORES + (CORES - 1 - c)

    def peer(d):
        return {"tp": ((x + d) % X) * CORES + c}

    def rows(j):
        return pl.ds(j * R, R)

    barrier = pltpu.get_barrier_semaphore()
    for d in range(1, X):
        pl.semaphore_signal(barrier, inc=1, device_id=peer(d), device_id_type=MESH)
    sides = (z > 0).astype(jnp.int32) + (z < Z - 1).astype(jnp.int32)

    def greet_sides(sem):
        @pl.when(z > 0)
        def _():
            pl.semaphore_signal(sem, inc=1, device_id={"sp": z - 1}, device_id_type=MESH)

        @pl.when(z < Z - 1)
        def _():
            pl.semaphore_signal(sem, inc=1, device_id={"sp": z + 1}, device_id_type=MESH)

    greet_sides(barrier)
    pl.semaphore_signal(barrier, inc=1, device_id={"tp": partner}, device_id_type=MESH)

    first = [pltpu.make_async_copy(tok_hbm.at[:, pl.ds(k * KC, KC)], raw.at[k], raw_sem.at[k]) for k in range(RAW)]
    loads = [pltpu.make_async_copy(tok_hbm.at[rows(j)], tok.at[rows(j)], loc_sem.at[j]) for j in range(blocks)]
    small = [
        pltpu.make_async_copy(src, dst, small_sem.at[i])
        for i, (src, dst) in enumerate(
            [(gain_hbm, gain_v), (gates_hbm, gates_v.at[0]), (q_hbm, q_v.at[0]), (nk_hbm, nk_v), (nv_hbm, nv_v), (ng_hbm, ng_v)]
        )
    ]
    for copy in first:
        copy.start()
    for copy in loads:
        copy.start()
    for copy in small:
        copy.start()
    w_copies = [
        pltpu.make_async_copy(src, wbuf.at[:, pl.ds(2 * i * C, C)], w_sem.at[i]) for i, src in enumerate((wk_hbm, wv_hbm))
    ]

    def to_partner(src, dst, i):
        return pltpu.make_async_remote_copy(
            src, dst, sw_sem.at[i], rw_sem.at[i], device_id={"tp": partner}, device_id_type=MESH
        )

    shares = [
        to_partner(wk_hbm, wbuf.at[:, pl.ds(C, C)], 0),
        to_partner(wv_hbm, wbuf.at[:, pl.ds(3 * C, C)], 1),
        to_partner(gates_hbm, gates_v.at[1], 2),
        to_partner(q_hbm, q_v.at[1], 3),
    ]

    def x_copy(d, k):
        src = raw.at[k] if isinstance(k, int) and k < RAW else nb.at[k]
        return pltpu.make_async_remote_copy(
            src, rx.at[d - 1, k], sx_sem.at[d - 1, k], rx_sem.at[d - 1, k], device_id=peer(d), device_id_type=MESH
        )

    def inv_copy(d):
        return pltpu.make_async_remote_copy(
            inv_tx, inv_rx.at[d - 1], si_sem.at[d - 1], ri_sem.at[d - 1], device_id=peer(d), device_id_type=MESH
        )

    def norm(v, r, k):
        return (v.astype(f32) * r * gain_row[:, pl.ds(k * KC, KC)]).astype(bf)

    for copy in first:
        copy.wait()
    pl.semaphore_wait(barrier, 1 + (X - 1) + sides)
    for k in range(RAW):
        for d in range(1, X):
            x_copy(d, k).start()

    small[0].wait()
    g = gain_v[...].astype(f32)
    lanes = g.shape[1]
    for i in range(g.shape[0]):
        gain_row[:, pl.ds(i * lanes, lanes)] = g[i : i + 1, :]
    for j in range(blocks):
        loads[j].wait()
        v = tok[rows(j), :].astype(f32)
        r = lax.rsqrt(jnp.mean(v * v, axis=-1, keepdims=True) + epsilon)
        inv[rows(j), :] = jnp.broadcast_to(r, (R, KC))
    for copy in w_copies:
        copy.start()
    eye = lax.broadcasted_iota(jnp.int32, (rows_each, rows_each), 0) == lax.broadcasted_iota(
        jnp.int32, (rows_each, rows_each), 1
    )
    inv_tx[...] = jnp.sum(jnp.where(eye, inv[:, :rows_each], 0.0), axis=0, keepdims=True)
    for k in range(RAW, NC):
        nb[k] = norm(tok[:, pl.ds(k * KC, KC)], inv[...], k)
        for d in range(1, X):
            x_copy(d, k).start()
        if k == RAW:
            for d in range(1, X):
                inv_copy(d).start()
    for copy in shares:
        copy.start()
    for k in range(RAW):
        nb[k] = norm(raw[k], inv[...], k)
    if Z > 2:
        greet_sides(hop_sem.at[0])

    for copy in small[1:]:
        copy.wait()
    for i in (2, 3):
        shares[i].wait_recv()

    scale = HD ** (-0.5)
    lane_head = lax.broadcasted_iota(jnp.int32, (C, C), 1) // HD
    same_head = lane_head == lax.broadcasted_iota(jnp.int32, (C, C), 0) // HD
    diagonal = lax.broadcasted_iota(jnp.int32, (C, C), 0) == lax.broadcasted_iota(jnp.int32, (C, C), 1)
    own_head = lax.broadcasted_iota(jnp.int32, (H, C), 1) // HD == lax.broadcasted_iota(jnp.int32, (H, C), 0)
    heads_eye = lax.broadcasted_iota(jnp.int32, (H, H), 0) == lax.broadcasted_iota(jnp.int32, (H, H), 1)
    last_block = z == Z - 1

    def as_row(column):
        return jnp.sum(jnp.where(own_head, column, 0.0), axis=0, keepdims=True)

    def source(d):
        return ((x + X - d) % X) * CORES + c

    for s in range(S):
        for g in range(CORES):
            column = jnp.sum(jnp.where(diagonal, q_v[g, s : s + 1, :].astype(f32), 0.0), axis=1, keepdims=True)
            qblock[s, g] = jnp.where(same_head, column, 0.0).astype(bf)
    head_of_lane = lax.broadcasted_iota(jnp.int32, (L, C), 1) // HD
    for d in range(X):
        pick = lax.broadcasted_iota(jnp.int32, (L, BL), 1) == lax.broadcasted_iota(
            jnp.int32, (L, BL), 0
        ) + source(d) * L
        for s in range(S):
            for g in range(CORES):
                spread = jnp.zeros((L, C), f32)
                for h in range(H):
                    column = jnp.sum(jnp.where(pick, gates_v[g, s, h : h + 1, :], 0.0), axis=1, keepdims=True)
                    spread = jnp.where(head_of_lane == h, column, spread)
                gate_rep[d, s, g] = spread
    for s in range(S):
        fresh = jnp.dot(nk_v[s : s + 1, :], qblock[s, 0], preferred_element_type=f32) * scale
        own_gate = jnp.sum(jnp.where(heads_eye, ng_v[s : s + 1, :], 0.0), axis=1, keepdims=True)
        fresh = jnp.where(last_block, fresh - as_row(gates_v[0, s, :, BL - 1 : BL] + own_gate), masked_score)
        weight = jnp.where(last_block, jnp.ones_like(fresh), 0.0)
        stats_tx[0, 0, s : s + 1, :] = fresh
        stats_tx[0, 1, s : s + 1, :] = weight
        stats_tx[0, 2, s : s + 1, :] = weight * nv_v[s : s + 1, :].astype(f32)
        stats_tx[1, 0, s : s + 1, :] = jnp.full((1, C), masked_score, f32)
        stats_tx[1, 1, s : s + 1, :] = jnp.zeros((1, C), f32)
        stats_tx[1, 2, s : s + 1, :] = jnp.zeros((1, C), f32)

    for d in range(1, X):
        inv_copy(d).wait_recv()
        r = jnp.sum(jnp.where(eye, inv_rx[d - 1], 0.0), axis=1, keepdims=True)
        for k in range(RAW):
            x_copy(d, k).wait_recv()
            rx[d - 1, k] = norm(rx[d - 1, k], r, k)

    def w_part(k):
        return wbuf[pl.ds(k * KC if isinstance(k, int) else pl.multiple_of(k * KC, KC), KC), :]

    def y_copy(d, s, v):
        at = pl.ds(pl.multiple_of(source(d) * L, L), L)
        return pltpu.make_async_remote_copy(
            ybuf.at[d, v, pl.ds(s * L, L)], (kbuf, vbuf)[v].at[s, at],
            sy_sem.at[d, s, v], ry_sem.at[d, s, v], device_id={"tp": partner}, device_id_type=MESH,
        )

    def y_arrival(d, s, v):
        at = pl.ds(pl.multiple_of(((x + X - d) % X * CORES + (CORES - 1 - c)) * L, L), L)
        return pltpu.make_async_remote_copy(
            ybuf.at[d, v, pl.ds(s * L, L)], (kbuf, vbuf)[v].at[s, at],
            sy_sem.at[d, s, v], ry_sem.at[d, s, v], device_id={"tp": partner}, device_id_type=MESH,
        )

    def finish(d, y, last):
        for s in range(S):
            at = pl.ds(s * L, L)
            for g in range(CORES):
                keys = y[s * L : (s + 1) * L, g * C : (g + 1) * C]
                values = y[s * L : (s + 1) * L, (2 + g) * C : (3 + g) * C].astype(f32)
                scores = jnp.dot(keys, qblock[s, g], preferred_element_type=f32) * scale - gate_rep[d, s, g]
                before = stats_tx[g, 0, s : s + 1, :]
                top = jnp.maximum(jnp.max(scores, axis=0, keepdims=True), before)
                weights = jnp.exp(scores - top)
                factor = jnp.exp(before - top)
                total = jnp.sum(weights, axis=0, keepdims=True) + factor * stats_tx[g, 1, s : s + 1, :]
                weighted = jnp.sum(weights * values, axis=0, keepdims=True) + factor * stats_tx[g, 2, s : s + 1, :]
                for i, row in enumerate((top, total, weighted)):
                    stats_tx[g, i, s : s + 1, :] = row
                    if last and g == 0:
                        stats_rx[z, 0, i, s : s + 1, :] = row

    def deliver(d, y):
        place = pl.ds(pl.multiple_of(source(d) * L, L), L)
        for s in range(S):
            part = y[s * L : (s + 1) * L]
            kbuf[s, place, :] = part[:, :C]
            vbuf[s, place, :] = part[:, 2 * C : 3 * C]
        ybuf[d, 0] = y[:, C : 2 * C]
        ybuf[d, 1] = y[:, 3 * C :]

    def send_partner(d):
        for s in range(S):
            for v in range(2):
                y_copy(d, s, v).start()

    for copy in w_copies:
        copy.wait()
    for i in (0, 1):
        shares[i].wait_recv()
    acc[...] = jnp.zeros_like(acc)

    def near(k, carry):
        acc[...] += jnp.dot(nb[k], w_part(k), preferred_element_type=f32)
        return carry

    lax.fori_loop(0, NC, near, 0)
    y = acc[...].astype(bf)
    deliver(0, y)
    finish(0, y, X == 1)
    send_partner(0)
    for r in range(1, Z - 2):
        pl.semaphore_wait(hop_sem.at[r - 1], sides)
        greet_sides(hop_sem.at[r])
    if Z > 2:
        pl.semaphore_wait(hop_sem.at[Z - 3], sides)
    pl.semaphore_signal(ready_sem, inc=1, device_id={"tp": partner}, device_id_type=MESH)
    pl.semaphore_wait(ready_sem, 1)

    for d in range(1, X):
        acc[...] = jnp.zeros_like(acc)

        def far(k, carry, d=d):
            @pl.when(k >= RAW)
            def _():
                x_copy(d, k).wait_recv()

            acc[...] += jnp.dot(rx[d - 1, k], w_part(k), preferred_element_type=f32)
            return carry

        lax.fori_loop(0, NC - 1, far, 0)
        x_copy(d, NC - 1).wait_recv()
        y = (acc[...] + jnp.dot(rx[d - 1, NC - 1], w_part(NC - 1), preferred_element_type=f32)).astype(bf)
        if d < X - 1:
            deliver(d, y)
            finish(d, y, False)
            send_partner(d)
        else:
            finish(d, y, True)

    def z_copy(d, other):
        return pltpu.make_async_remote_copy(
            stats_tx.at[other], stats_rx.at[z, other], sz_sem.at[other, d], rz_sem.at[other, d],
            device_id={"sp": (z + d) % Z, "tp": partner if other else tp}, device_id_type=MESH,
        )

    sends = [(d, other) for other in range(CORES) for d in range(Z) if d or other]
    for d, other in sorted(sends, key=lambda e: -min(e[0], Z - e[0])):
        z_copy(d, other).start()
    if X > 1:
        deliver(X - 1, y)
        send_partner(X - 1)
    for d in range(1, X):
        inv_copy(d).wait_send()
        for k in range(NC):
            x_copy(d, k).wait_send()
    for copy in shares:
        copy.wait_send()
    for d in range(X):
        for s in range(S):
            for v in range(2):
                y_copy(d, s, v).wait_send()
                y_arrival(d, s, v).wait_recv()
    for d, other in sends:
        at = (z + Z - d) % Z
        pltpu.make_async_remote_copy(
            stats_tx.at[other], stats_rx.at[at, other], sz_sem.at[other, d], rz_sem.at[other, d],
            device_id={"sp": at, "tp": partner if other else tp}, device_id_type=MESH,
        ).wait_recv()
    everything = stats_rx[...].reshape(Z * CORES, 3, S, C)
    tops, totals, sums = everything[:, 0], everything[:, 1], everything[:, 2]
    factor = jnp.exp(tops - jnp.max(tops, axis=0, keepdims=True))
    ro_ref[...] = (jnp.sum(sums * factor, axis=0) / jnp.sum(totals * factor, axis=0)).astype(ro_ref.dtype)
    for d, other in sends:
        z_copy(d, other).wait_send()


def write_out(*refs):
    sems = refs[-1]
    count = (len(refs) - 1) // 2
    copies = [pltpu.make_async_copy(refs[i], refs[count + i], sems.at[i]) for i in range(count)]
    for copy in copies:
        copy.start()
    for copy in copies:
        copy.wait()


def body(
    tokens, norm_gain, key_weight, value_weight, cum_gates, new_query, new_key, new_value, new_gate
):
    S, L, D = tokens.shape
    C = key_weight.shape[1]
    H = C // HD
    T = lax.axis_size("tp")
    Z = lax.axis_size("sp")
    X = T // CORES
    BL = T * L
    R = 16 if L % 16 == 0 else L
    KC = 256 if D % 256 == 0 else D // 2
    NC = D // KC
    bf, f32 = jnp.bfloat16, jnp.float32
    hbm = pl.BlockSpec(memory_space=pltpu.HBM)
    dma = pltpu.SemaphoreType.DMA
    regular = pltpu.SemaphoreType.REGULAR
    far = max(X - 1, 1)
    vmem = pl.BlockSpec(memory_space=pltpu.VMEM)
    results = pl.pallas_call(
        functools.partial(kernel, (S, L, R, T, Z)),
        out_shape=(
            pltpu.VMEM((S, BL, C), bf),
            pltpu.VMEM((S, BL, C), bf),
            pltpu.VMEM((S, C), bf),
        ),
        in_specs=[hbm] * 9,
        out_specs=(vmem, vmem, vmem),
        scratch_shapes=[
            pltpu.VMEM((S * L, D), bf),
            pltpu.VMEM((RAW, S * L, KC), bf),
            pltpu.VMEM((S * L, KC), f32),
            pltpu.VMEM((NC, S * L, KC), bf),
            pltpu.VMEM((far, NC, S * L, KC), bf),
            pltpu.VMEM((S * L, 4 * C), f32),
            pltpu.VMEM((D, 4 * C), bf),
            pltpu.VMEM((X, 2, S * L, C), bf),
            pltpu.VMEM((D // 128, 128), bf),
            pltpu.VMEM((1, D), f32),
            pltpu.VMEM((CORES, S, H, BL), f32),
            pltpu.VMEM((CORES, S, C), bf),
            pltpu.VMEM((S, C), bf),
            pltpu.VMEM((S, C), bf),
            pltpu.VMEM((S, H), f32),
            pltpu.VMEM((1, S * L), f32),
            pltpu.VMEM((far, 1, S * L), f32),
            pltpu.VMEM((S, CORES, C, C), bf),
            pltpu.VMEM((X, S, CORES, L, C), f32),
            pltpu.VMEM((CORES, 3, S, C), f32),
            pltpu.VMEM((Z, CORES, 3, S, C), f32),
            dma((S * L // R,)), dma((RAW,)), dma((2,)), dma((6,)), regular((max(Z - 2, 1),)), regular,
            dma((far, NC)), dma((far, NC)), dma((far,)), dma((far,)), dma((4,)), dma((4,)),
            dma((X, S, 2)), dma((X, S, 2)), dma((CORES, Z)), dma((CORES, Z)),
        ],
        compiler_params=pltpu.CompilerParams(
            collective_id=0, has_side_effects=True, vmem_limit_bytes=56 * 1024 * 1024
        ),
    )(
        tokens.reshape(S * L, D),
        norm_gain.reshape(D // 128, 128),
        key_weight,
        value_weight,
        jnp.transpose(cum_gates, (0, 2, 1)),
        new_query,
        new_key,
        new_value,
        new_gate,
    )
    return pl.pallas_call(
        write_out,
        out_shape=tuple(jax.ShapeDtypeStruct(r.shape, r.dtype) for r in results),
        in_specs=[vmem] * 3,
        out_specs=(hbm, hbm, hbm),
        scratch_shapes=[dma((3,))],
    )(*(pltpu.with_memory_space_constraint(r, pltpu.VMEM) for r in results))


def solution(mesh):
    in_specs = (
        P("gr", ("sp", "tp"), None),
        P(),
        P(None, "tp"),
        P(None, "tp"),
        P("gr", "sp", "tp"),
        P("gr", "tp"),
        P("gr", "tp"),
        P("gr", "tp"),
        P("gr", "tp"),
    )
    out_specs = (P("gr", "sp", "tp"), P("gr", "sp", "tp"), P("gr", "tp"))
    return jax.shard_map(body, mesh=mesh, in_specs=in_specs, out_specs=out_specs, check_vma=False)
```

time: 37 us -> 35.9 us (0.970)
  Pallas kernels: 36.3 us -> 35.1 us
    pallas_call x1, Pallas kernels: 35.4 us -> 34.3 us  [body(): pl.pallas_call(functools.partial(kernel, (S, L, R, T, Z)), out_shape=(plt...]
where the time goes in v1:
time: 35.9 us; the launch traced here: 35.7 us
  Pallas kernels  35.1 us (98%)
  between operations  0.64 us (2%)
    pallas_call x1, Pallas kernels, body(): pl.pallas_call(functools.partial(kernel, (S, L, R, T, Z)), out_shape=(plt...  34.3 us
    pallas_call x1, Pallas kernels, body(): pl.pallas_call(write_out, out_shape=tuple((jax.ShapeDtypeStruct(r.shape,...  0.82 us

profile of v1, /device:TPU:0, one launch (start us, length us, event | category | flops | bytes accessed | tf_op | source)
XLA Modules:
  0.0 35.7 jit_solution(6860405165366675681)
XLA Ops:
  0.6 34.3 %shard_map.112 = (bf16[2,256,256]{2,1,0:T(8,128)(2,1)S(1)}, bf16[2,256,256]{2,1,0:T(8,128)(2,1)S(1)}, bf16[2,256]{1,0:T(2,128)(2,1)S(1)}) custom-call(bf16[128,4096]{1,0:T(8,128)(2,1)} %bitcast.3, bf16[32,128]{1,0:T(8,128)(2,1)} %bitcast.4, bf16[4096,256]{1,0:T(8,128)(2,1)} %wk_hbm.1, bf16[4096,256]{1,0:T(8,128)(2,1)} %wv_hbm.1, f32[2,4,256]{2,1,0:T(4,128)} %bitcast.5, ...), custom_call_target="tpu_custom_call" | custom-call | tf_op jit(solution)/shard_map/pallas_call | solution.py:359
  34.9 0.8 %shard_map.113 = (bf16[2,256,256]{2,1,0:T(8,128)(2,1)}, bf16[2,256,256]{2,1,0:T(8,128)(2,1)}, bf16[2,256]{1,0:T(2,128)(2,1)}) custom-call(bf16[2,256,256]{2,1,0:T(8,128)(2,1)S(1)} %get-tuple-element.6.refs_0_, bf16[2,256,256]{2,1,0:T(8,128)(2,1)S(1)} %get-tuple-element.7.refs_1_, bf16[2,256]{1,0:T(2,128)(2,1)S(1)} %get-tuple-element.8.refs_2_), custom_call_target="tpu_custom_call" | custom-call | tf_op jit(solution)/shard_map/pallas_call | solution.py:408

commit v2 on v1

--- a/solution.py
+++ b/solution.py
@@ -9,7 +9,8 @@
 
 HD = 64
 CORES = 2
-RAW = 1
+LEAD = 4
+RAW = 2
 
 epsilon = 1e-06
 masked_score = -1e30
@@ -20,7 +21,7 @@
     dims,
     tok_hbm, gain_hbm, wk_hbm, wv_hbm, gates_hbm, q_hbm, nk_hbm, nv_hbm, ng_hbm,
     kbuf, vbuf, ro_ref,
-    tok, raw, inv, nb, rx, acc, wbuf, ybuf, gain_v, gain_row, gates_v, q_v, nk_v, nv_v, ng_v,
+    tok, raw, inv, nb, rx, acc, wbuf, ybuf, gain_v, gain_row, gates_v, new_v, ng_v,
     inv_tx, inv_rx, qblock, gate_rep, stats_tx, stats_rx,
     loc_sem, raw_sem, w_sem, small_sem, hop_sem, ready_sem,
     sx_sem, rx_sem, si_sem, ri_sem, sw_sem, rw_sem, sy_sem, ry_sem, sz_sem, rz_sem,
@@ -45,6 +46,9 @@
     def rows(j):
         return pl.ds(j * R, R)
 
+    first = [pltpu.make_async_copy(tok_hbm.at[:, pl.ds(k * KC, KC)], raw.at[k], raw_sem) for k in range(RAW)]
+    for copy in first:
+        copy.start()
     barrier = pltpu.get_barrier_semaphore()
     for d in range(1, X):
         pl.semaphore_signal(barrier, inc=1, device_id=peer(d), device_id_type=MESH)
@@ -62,22 +66,19 @@
     greet_sides(barrier)
     pl.semaphore_signal(barrier, inc=1, device_id={"tp": partner}, device_id_type=MESH)
 
-    first = [pltpu.make_async_copy(tok_hbm.at[:, pl.ds(k * KC, KC)], raw.at[k], raw_sem.at[k]) for k in range(RAW)]
     loads = [pltpu.make_async_copy(tok_hbm.at[rows(j)], tok.at[rows(j)], loc_sem.at[j]) for j in range(blocks)]
     small = [
-        pltpu.make_async_copy(src, dst, small_sem.at[i])
+        pltpu.make_async_copy(src, dst, small_sem.at[min(i, 3)])
         for i, (src, dst) in enumerate(
-            [(gain_hbm, gain_v), (gates_hbm, gates_v.at[0]), (q_hbm, q_v.at[0]), (nk_hbm, nk_v), (nv_hbm, nv_v), (ng_hbm, ng_v)]
+            [(gain_hbm, gain_v), (gates_hbm, gates_v.at[0]), (ng_hbm, ng_v), (q_hbm, new_v.at[0]), (nk_hbm, new_v.at[1]), (nv_hbm, new_v.at[2])]
         )
     ]
-    for copy in first:
-        copy.start()
     for copy in loads:
         copy.start()
     for copy in small:
         copy.start()
     w_copies = [
-        pltpu.make_async_copy(src, wbuf.at[:, pl.ds(2 * i * C, C)], w_sem.at[i]) for i, src in enumerate((wk_hbm, wv_hbm))
+        pltpu.make_async_copy(src, wbuf.at[:, pl.ds(2 * i * C, C)], w_sem) for i, src in enumerate((wk_hbm, wv_hbm))
     ]
 
     def to_partner(src, dst, i):
@@ -87,15 +88,27 @@
 
     shares = [
         to_partner(wk_hbm, wbuf.at[:, pl.ds(C, C)], 0),
-        to_partner(wv_hbm, wbuf.at[:, pl.ds(3 * C, C)], 1),
-        to_partner(gates_hbm, gates_v.at[1], 2),
-        to_partner(q_hbm, q_v.at[1], 3),
+        to_partner(wv_hbm, wbuf.at[:, pl.ds(3 * C, C)], 0),
+        to_partner(gates_hbm, gates_v.at[1], 1),
+        to_partner(q_hbm, new_v.at[3], 2),
     ]
+    both_weights = to_partner(wbuf.at[:, pl.ds(0, 2 * C)], wbuf.at[:, pl.ds(0, 2 * C)], 0)
+
+    groups = [(0, RAW)] + [g for g in ((RAW, NC // 2), (NC // 2, NC - 2), (NC - 2, NC - 1)) if g[0] < g[1]] + [(NC - 1, NC)]
+
+    def group_of(k):
+        return next(i for i, (a, b) in enumerate(groups) if a <= k < b)
 
     def x_copy(d, k):
-        src = raw.at[k] if isinstance(k, int) and k < RAW else nb.at[k]
-        return pltpu.make_async_remote_copy(
-            src, rx.at[d - 1, k], sx_sem.at[d - 1, k], rx_sem.at[d - 1, k], device_id=peer(d), device_id_type=MESH
+        src = raw.at[k] if k < RAW else nb.at[k]
+        return pltpu.make_async_remote_copy(
+            src, rx.at[d - 1, k], sx_sem.at[d - 1], rx_sem.at[d - 1, group_of(k)], device_id=peer(d), device_id_type=MESH
+        )
+
+    def x_whole(d, first, count, group):
+        part = rx.at[d - 1, pl.ds(first, count)]
+        return pltpu.make_async_remote_copy(
+            part, part, sx_sem.at[d - 1], rx_sem.at[d - 1, group], device_id=peer(d), device_id_type=MESH
         )
 
     def inv_copy(d):
@@ -106,12 +119,16 @@
     def norm(v, r, k):
         return (v.astype(f32) * r * gain_row[:, pl.ds(k * KC, KC)]).astype(bf)
 
-    for copy in first:
-        copy.wait()
+    pltpu.make_async_copy(raw, raw, raw_sem).wait()
     pl.semaphore_wait(barrier, 1 + (X - 1) + sides)
-    for k in range(RAW):
-        for d in range(1, X):
-            x_copy(d, k).start()
+
+    def send(chunks):
+        for k in chunks:
+            for d in range(1, X):
+                x_copy(d, k).start()
+
+    pl.when(c == 0)(lambda: send(range(RAW)))
+    pl.when(c != 0)(lambda: send(range(RAW)))
 
     small[0].wait()
     g = gain_v[...].astype(f32)
@@ -131,20 +148,28 @@
     inv_tx[...] = jnp.sum(jnp.where(eye, inv[:, :rows_each], 0.0), axis=0, keepdims=True)
     for k in range(RAW, NC):
         nb[k] = norm(tok[:, pl.ds(k * KC, KC)], inv[...], k)
-        for d in range(1, X):
-            x_copy(d, k).start()
+        if k < LEAD:
+            send([k])
+        else:
+            pl.when(c == 0)(lambda k=k: send([k]))
         if k == RAW:
             for d in range(1, X):
                 inv_copy(d).start()
-    for copy in shares:
+    for copy in shares[2:] + shares[:2]:
         copy.start()
     for k in range(RAW):
         nb[k] = norm(raw[k], inv[...], k)
     if Z > 2:
         greet_sides(hop_sem.at[0])
 
-    for copy in small[1:]:
-        copy.wait()
+    @pl.when(c != 0)
+    def _():
+        for d in range(1, X):
+            x_whole(d, 0, LEAD, 0).wait_send()
+
+    small[1].wait()
+    small[2].wait()
+    pltpu.make_async_copy(new_v.at[pl.ds(0, 3)], new_v.at[pl.ds(0, 3)], small_sem.at[3]).wait()
     for i in (2, 3):
         shares[i].wait_recv()
 
@@ -164,7 +189,7 @@
 
     for s in range(S):
         for g in range(CORES):
-            column = jnp.sum(jnp.where(diagonal, q_v[g, s : s + 1, :].astype(f32), 0.0), axis=1, keepdims=True)
+            column = jnp.sum(jnp.where(diagonal, new_v[3 * g, s : s + 1, :].astype(f32), 0.0), axis=1, keepdims=True)
             qblock[s, g] = jnp.where(same_head, column, 0.0).astype(bf)
     head_of_lane = lax.broadcasted_iota(jnp.int32, (L, C), 1) // HD
     for d in range(X):
@@ -179,22 +204,23 @@
                     spread = jnp.where(head_of_lane == h, column, spread)
                 gate_rep[d, s, g] = spread
     for s in range(S):
-        fresh = jnp.dot(nk_v[s : s + 1, :], qblock[s, 0], preferred_element_type=f32) * scale
+        fresh = jnp.dot(new_v[1, s : s + 1, :], qblock[s, 0], preferred_element_type=f32) * scale
         own_gate = jnp.sum(jnp.where(heads_eye, ng_v[s : s + 1, :], 0.0), axis=1, keepdims=True)
         fresh = jnp.where(last_block, fresh - as_row(gates_v[0, s, :, BL - 1 : BL] + own_gate), masked_score)
         weight = jnp.where(last_block, jnp.ones_like(fresh), 0.0)
         stats_tx[0, 0, s : s + 1, :] = fresh
         stats_tx[0, 1, s : s + 1, :] = weight
-        stats_tx[0, 2, s : s + 1, :] = weight * nv_v[s : s + 1, :].astype(f32)
+        stats_tx[0, 2, s : s + 1, :] = weight * new_v[2, s : s + 1, :].astype(f32)
         stats_tx[1, 0, s : s + 1, :] = jnp.full((1, C), masked_score, f32)
         stats_tx[1, 1, s : s + 1, :] = jnp.zeros((1, C), f32)
         stats_tx[1, 2, s : s + 1, :] = jnp.zeros((1, C), f32)
 
+    pl.when(c != 0)(lambda: send(range(LEAD, NC)))
     for d in range(1, X):
         inv_copy(d).wait_recv()
         r = jnp.sum(jnp.where(eye, inv_rx[d - 1], 0.0), axis=1, keepdims=True)
+        x_whole(d, 0, RAW, 0).wait_recv()
         for k in range(RAW):
-            x_copy(d, k).wait_recv()
             rx[d - 1, k] = norm(rx[d - 1, k], r, k)
 
     def w_part(k):
@@ -204,33 +230,33 @@
         at = pl.ds(pl.multiple_of(source(d) * L, L), L)
         return pltpu.make_async_remote_copy(
             ybuf.at[d, v, pl.ds(s * L, L)], (kbuf, vbuf)[v].at[s, at],
-            sy_sem.at[d, s, v], ry_sem.at[d, s, v], device_id={"tp": partner}, device_id_type=MESH,
-        )
-
-    def y_arrival(d, s, v):
-        at = pl.ds(pl.multiple_of(((x + X - d) % X * CORES + (CORES - 1 - c)) * L, L), L)
-        return pltpu.make_async_remote_copy(
-            ybuf.at[d, v, pl.ds(s * L, L)], (kbuf, vbuf)[v].at[s, at],
-            sy_sem.at[d, s, v], ry_sem.at[d, s, v], device_id={"tp": partner}, device_id_type=MESH,
+            sy_sem, ry_sem, device_id={"tp": partner}, device_id_type=MESH,
         )
 
     def finish(d, y, last):
-        for s in range(S):
-            at = pl.ds(s * L, L)
-            for g in range(CORES):
-                keys = y[s * L : (s + 1) * L, g * C : (g + 1) * C]
-                values = y[s * L : (s + 1) * L, (2 + g) * C : (3 + g) * C].astype(f32)
-                scores = jnp.dot(keys, qblock[s, g], preferred_element_type=f32) * scale - gate_rep[d, s, g]
-                before = stats_tx[g, 0, s : s + 1, :]
-                top = jnp.maximum(jnp.max(scores, axis=0, keepdims=True), before)
-                weights = jnp.exp(scores - top)
-                factor = jnp.exp(before - top)
-                total = jnp.sum(weights, axis=0, keepdims=True) + factor * stats_tx[g, 1, s : s + 1, :]
-                weighted = jnp.sum(weights * values, axis=0, keepdims=True) + factor * stats_tx[g, 2, s : s + 1, :]
-                for i, row in enumerate((top, total, weighted)):
-                    stats_tx[g, i, s : s + 1, :] = row
-                    if last and g == 0:
-                        stats_rx[z, 0, i, s : s + 1, :] = row
+        pairs = [(g, s) for g in range(CORES) for s in range(S)]
+        before = {(g, s): [stats_tx[g, i, s : s + 1, :] for i in range(3)] for g, s in pairs}
+        scores = {}
+        for g, s in pairs:
+            keys = y[s * L : (s + 1) * L, g * C : (g + 1) * C]
+            scores[g, s] = jnp.dot(keys, qblock[s, g], preferred_element_type=f32) * scale - gate_rep[d, s, g]
+        after = {}
+        for g, s in pairs:
+            old_top, old_total, old_weighted = before[g, s]
+            values = y[s * L : (s + 1) * L, (2 + g) * C : (3 + g) * C].astype(f32)
+            top = jnp.maximum(jnp.max(scores[g, s], axis=0, keepdims=True), old_top)
+            weights = jnp.exp(scores[g, s] - top)
+            factor = jnp.exp(old_top - top)
+            total = jnp.sum(weights, axis=0, keepdims=True) + factor * old_total
+            weighted = jnp.sum(weights * values, axis=0, keepdims=True) + factor * old_weighted
+            after[g, s] = (top, total, weighted)
+        for g, s in pairs:
+            for i, row in enumerate(after[g, s]):
+                stats_tx[g, i, s : s + 1, :] = row
+        if last:
+            for s in range(S):
+                for i, row in enumerate(after[0, s]):
+                    stats_rx[0, z, i, s : s + 1, :] = row
 
     def deliver(d, y):
         place = pl.ds(pl.multiple_of(source(d) * L, L), L)
@@ -246,10 +272,8 @@
             for v in range(2):
                 y_copy(d, s, v).start()
 
-    for copy in w_copies:
-        copy.wait()
-    for i in (0, 1):
-        shares[i].wait_recv()
+    pltpu.make_async_copy(wbuf.at[:, pl.ds(0, 2 * C)], wbuf.at[:, pl.ds(0, 2 * C)], w_sem).wait()
+    both_weights.wait_recv()
     acc[...] = jnp.zeros_like(acc)
 
     def near(k, carry):
@@ -273,15 +297,14 @@
         acc[...] = jnp.zeros_like(acc)
 
         def far(k, carry, d=d):
-            @pl.when(k >= RAW)
-            def _():
-                x_copy(d, k).wait_recv()
-
             acc[...] += jnp.dot(rx[d - 1, k], w_part(k), preferred_element_type=f32)
             return carry
 
-        lax.fori_loop(0, NC - 1, far, 0)
-        x_copy(d, NC - 1).wait_recv()
+        for i, (start, stop) in enumerate(groups[:-1]):
+            if i:
+                x_whole(d, start, stop - start, i).wait_recv()
+            lax.fori_loop(start, stop, far, 0)
+        x_whole(d, NC - 1, 1, len(groups) - 1).wait_recv()
         y = (acc[...] + jnp.dot(rx[d - 1, NC - 1], w_part(NC - 1), preferred_element_type=f32)).astype(bf)
         if d < X - 1:
             deliver(d, y)
@@ -290,41 +313,61 @@
         else:
             finish(d, y, True)
 
-    def z_copy(d, other):
-        return pltpu.make_async_remote_copy(
-            stats_tx.at[other], stats_rx.at[z, other], sz_sem.at[other, d], rz_sem.at[other, d],
-            device_id={"sp": (z + d) % Z, "tp": partner if other else tp}, device_id_type=MESH,
-        )
-
-    sends = [(d, other) for other in range(CORES) for d in range(Z) if d or other]
-    for d, other in sorted(sends, key=lambda e: -min(e[0], Z - e[0])):
-        z_copy(d, other).start()
+    def z_target(i):
+        return jnp.where(2 * z >= Z, i, Z - 1 - i)
+
+    def z_copy(i, other):
+        to = z_target(i)
+        return pltpu.make_async_remote_copy(
+            stats_tx.at[other], stats_rx.at[other, z], sz_sem.at[other], rz_sem.at[other],
+            device_id={"sp": to, "tp": partner if other else tp}, device_id_type=MESH,
+        )
+
+    for i in range(Z):
+        for first_core in range(CORES):
+
+            @pl.when(c == first_core)
+            def _(i=i, first_core=first_core):
+                for core in range(CORES):
+                    if core == first_core:
+                        pl.when(z_target(i) != z)(z_copy(i, 0).start)
+                    else:
+                        z_copy(i, 1).start()
+
     if X > 1:
         deliver(X - 1, y)
         send_partner(X - 1)
     for d in range(1, X):
         inv_copy(d).wait_send()
-        for k in range(NC):
-            x_copy(d, k).wait_send()
-    for copy in shares:
-        copy.wait_send()
-    for d in range(X):
-        for s in range(S):
-            for v in range(2):
-                y_copy(d, s, v).wait_send()
-                y_arrival(d, s, v).wait_recv()
-    for d, other in sends:
-        at = (z + Z - d) % Z
-        pltpu.make_async_remote_copy(
-            stats_tx.at[other], stats_rx.at[at, other], sz_sem.at[other, d], rz_sem.at[other, d],
-            device_id={"sp": at, "tp": partner if other else tp}, device_id_type=MESH,
-        ).wait_recv()
-    everything = stats_rx[...].reshape(Z * CORES, 3, S, C)
-    tops, totals, sums = everything[:, 0], everything[:, 1], everything[:, 2]
-    factor = jnp.exp(tops - jnp.max(tops, axis=0, keepdims=True))
-    ro_ref[...] = (jnp.sum(sums * factor, axis=0) / jnp.sum(totals * factor, axis=0)).astype(ro_ref.dtype)
-    for d, other in sends:
-        z_copy(d, other).wait_send()
+        pl.when(c == 0)(x_whole(d, 0, NC, 0).wait_send)
+        pl.when(c != 0)(x_whole(d, LEAD, NC - LEAD, 0).wait_send)
+    both_weights.wait_send()
+    shares[2].wait_send()
+    shares[3].wait_send()
+    halves = pltpu.make_async_remote_copy(ybuf, ybuf, sy_sem, ry_sem, device_id={"tp": partner}, device_id_type=MESH)
+    halves.wait_send()
+    halves.wait_recv()
+
+    def z_whole(other):
+        part = stats_rx.at[other, pl.ds(0, Z - 1 + other)]
+        return pltpu.make_async_remote_copy(
+            part, part, sz_sem.at[other], rz_sem.at[other],
+            device_id={"tp": partner if other else tp}, device_id_type=MESH,
+        )
+
+    for other in range(CORES):
+        if Z - 1 + other:
+            z_whole(other).wait_recv()
+    entries = [(i, other) for i in range(Z) for other in range(CORES)]
+    tops = [stats_rx[other, i, 0] for i, other in entries]
+    most = functools.reduce(jnp.maximum, tops)
+    factors = [jnp.exp(top - most) for top in tops]
+    total = functools.reduce(jnp.add, [f * stats_rx[other, i, 1] for f, (i, other) in zip(factors, entries)])
+    weighted = functools.reduce(jnp.add, [f * stats_rx[other, i, 2] for f, (i, other) in zip(factors, entries)])
+    ro_ref[...] = (weighted / total).astype(ro_ref.dtype)
+    for other in range(CORES):
+        if Z - 1 + other:
+            z_whole(other).wait_send()
 
 
 def write_out(*refs):
@@ -347,7 +390,7 @@
     Z = lax.axis_size("sp")
     X = T // CORES
     BL = T * L
-    R = 16 if L % 16 == 0 else L
+    R = 32 if L % 32 == 0 else L
     KC = 256 if D % 256 == 0 else D // 2
     NC = D // KC
     bf, f32 = jnp.bfloat16, jnp.float32
@@ -377,19 +420,17 @@
             pltpu.VMEM((D // 128, 128), bf),
             pltpu.VMEM((1, D), f32),
             pltpu.VMEM((CORES, S, H, BL), f32),
-            pltpu.VMEM((CORES, S, C), bf),
-            pltpu.VMEM((S, C), bf),
-            pltpu.VMEM((S, C), bf),
+            pltpu.VMEM((4, S, C), bf),
             pltpu.VMEM((S, H), f32),
             pltpu.VMEM((1, S * L), f32),
             pltpu.VMEM((far, 1, S * L), f32),
             pltpu.VMEM((S, CORES, C, C), bf),
             pltpu.VMEM((X, S, CORES, L, C), f32),
             pltpu.VMEM((CORES, 3, S, C), f32),
-            pltpu.VMEM((Z, CORES, 3, S, C), f32),
-            dma((S * L // R,)), dma((RAW,)), dma((2,)), dma((6,)), regular((max(Z - 2, 1),)), regular,
-            dma((far, NC)), dma((far, NC)), dma((far,)), dma((far,)), dma((4,)), dma((4,)),
-            dma((X, S, 2)), dma((X, S, 2)), dma((CORES, Z)), dma((CORES, Z)),
+            pltpu.VMEM((CORES, Z, 3, S, C), f32),
+            dma((S * L // R,)), dma, dma, dma((4,)), regular((max(Z - 2, 1),)), regular,
+            dma((far,)), dma((far, 5)), dma((far,)), dma((far,)), dma((3,)), dma((3,)),
+            dma, dma, dma((CORES,)), dma((CORES,)),
         ],
         compiler_params=pltpu.CompilerParams(
             collective_id=0, has_side_effects=True, vmem_limit_bytes=56 * 1024 * 1024

time: 35.9 us -> 34.3 us (0.955)
  Pallas kernels: 35.1 us -> 33.5 us
    pallas_call x1, Pallas kernels: 34.3 us -> 32.7 us  [body(): pl.pallas_call(functools.partial(kernel, (S, L, R, T, Z)), out_shape=(plt...]
where the time goes in v2:
time: 34.3 us; the launch traced here: 34.2 us
  Pallas kernels  33.5 us (98%)
  between operations  0.64 us (2%)
    pallas_call x1, Pallas kernels, body(): pl.pallas_call(functools.partial(kernel, (S, L, R, T, Z)), out_shape=(plt...  32.7 us
    pallas_call x1, Pallas kernels, body(): pl.pallas_call(write_out, out_shape=tuple((jax.ShapeDtypeStruct(r.shape,...  0.82 us

profile of v2, /device:TPU:0, one launch (start us, length us, event | category | flops | bytes accessed | tf_op | source)
XLA Modules:
  0.0 34.2 jit_solution(12537754176984394822)
XLA Ops:
  0.6 32.7 %shard_map.112 = (bf16[2,256,256]{2,1,0:T(8,128)(2,1)S(1)}, bf16[2,256,256]{2,1,0:T(8,128)(2,1)S(1)}, bf16[2,256]{1,0:T(2,128)(2,1)S(1)}) custom-call(bf16[128,4096]{1,0:T(8,128)(2,1)} %bitcast.3, bf16[32,128]{1,0:T(8,128)(2,1)} %bitcast.4, bf16[4096,256]{1,0:T(8,128)(2,1)} %wk_hbm.1, bf16[4096,256]{1,0:T(8,128)(2,1)} %wv_hbm.1, f32[2,4,256]{2,1,0:T(4,128)} %bitcast.5, ...), custom_call_target="tpu_custom_call" | custom-call | tf_op jit(solution)/shard_map/pallas_call | solution.py:402
  33.4 0.8 %shard_map.113 = (bf16[2,256,256]{2,1,0:T(8,128)(2,1)}, bf16[2,256,256]{2,1,0:T(8,128)(2,1)}, bf16[2,256]{1,0:T(2,128)(2,1)}) custom-call(bf16[2,256,256]{2,1,0:T(8,128)(2,1)S(1)} %get-tuple-element.6.refs_0_, bf16[2,256,256]{2,1,0:T(8,128)(2,1)S(1)} %get-tuple-element.7.refs_1_, bf16[2,256]{1,0:T(2,128)(2,1)S(1)} %get-tuple-element.8.refs_2_), custom_call_target="tpu_custom_call" | custom-call | tf_op jit(solution)/shard_map/pallas_call | solution.py:449

commit v3 on v2

--- a/solution.py
+++ b/solution.py
@@ -10,6 +10,7 @@
 HD = 64
 CORES = 2
 LEAD = 4
+EXTRA = 8
 RAW = 2
 
 epsilon = 1e-06
@@ -22,9 +23,10 @@
     tok_hbm, gain_hbm, wk_hbm, wv_hbm, gates_hbm, q_hbm, nk_hbm, nv_hbm, ng_hbm,
     kbuf, vbuf, ro_ref,
     tok, raw, inv, nb, rx, acc, wbuf, ybuf, gain_v, gain_row, gates_v, new_v, ng_v,
-    inv_tx, inv_rx, qblock, gate_rep, stats_tx, stats_rx,
-    loc_sem, raw_sem, w_sem, small_sem, hop_sem, ready_sem,
+    inv_tx, inv_rx, qblock, gate_rep, stats_tx, stats_rx, lent, lent_tx, lent_rx,
+    loc_sem, raw_sem, w_sem, small_sem, hop_sem, answer_sem, ready_sem,
     sx_sem, rx_sem, si_sem, ri_sem, sw_sem, rw_sem, sy_sem, ry_sem, sz_sem, rz_sem,
+    sl_sem, rl_sem, sf_sem, rf_sem, sg_sem, rg_sem, sk_sem, rk_sem,
 ):
     S, L, R, T, Z = dims
     X = T // CORES
@@ -35,9 +37,14 @@
     C = kbuf.shape[2]
     H = C // HD
     BL = T * L
+    E = EXTRA
+    kept = rows_each - E
     tp = lax.axis_index("tp")
     z = lax.axis_index("sp")
     x, c = tp // CORES, tp % CORES
+    lender, helper = z == Z - 1, z == 0
+    if Z == 1:
+        lender = helper = z < 0
     partner = x * CORES + (CORES - 1 - c)
 
     def peer(d):
@@ -49,6 +56,7 @@
     first = [pltpu.make_async_copy(tok_hbm.at[:, pl.ds(k * KC, KC)], raw.at[k], raw_sem) for k in range(RAW)]
     for copy in first:
         copy.start()
+    rx[:, :, kept:, :] = jnp.zeros((rx.shape[0], NC, 2 * E, KC), bf)
     barrier = pltpu.get_barrier_semaphore()
     for d in range(1, X):
         pl.semaphore_signal(barrier, inc=1, device_id=peer(d), device_id_type=MESH)
@@ -63,7 +71,10 @@
         def _():
             pl.semaphore_signal(sem, inc=1, device_id={"sp": z + 1}, device_id_type=MESH)
 
-    greet_sides(barrier)
+    @pl.when(z < Z - 1)
+    def _():
+        pl.semaphore_signal(barrier, inc=1, device_id={"sp": z + 1}, device_id_type=MESH)
+
     pl.semaphore_signal(barrier, inc=1, device_id={"tp": partner}, device_id_type=MESH)
 
     loads = [pltpu.make_async_copy(tok_hbm.at[rows(j)], tok.at[rows(j)], loc_sem.at[j]) for j in range(blocks)]
@@ -94,21 +105,57 @@
     ]
     both_weights = to_partner(wbuf.at[:, pl.ds(0, 2 * C)], wbuf.at[:, pl.ds(0, 2 * C)], 0)
 
-    groups = [(0, RAW)] + [g for g in ((RAW, NC // 2), (NC // 2, NC - 2), (NC - 2, NC - 1)) if g[0] < g[1]] + [(NC - 1, NC)]
-
-    def group_of(k):
-        return next(i for i, (a, b) in enumerate(groups) if a <= k < b)
-
-    def x_copy(d, k):
-        src = raw.at[k] if k < RAW else nb.at[k]
-        return pltpu.make_async_remote_copy(
-            src, rx.at[d - 1, k], sx_sem.at[d - 1], rx_sem.at[d - 1, group_of(k)], device_id=peer(d), device_id_type=MESH
-        )
-
-    def x_whole(d, first, count, group):
-        part = rx.at[d - 1, pl.ds(first, count)]
-        return pltpu.make_async_remote_copy(
-            part, part, sx_sem.at[d - 1], rx_sem.at[d - 1, group], device_id=peer(d), device_id_type=MESH
+    HALF = NC // 2
+
+    def x_copy(d, k, count=rows_each):
+        return pltpu.make_async_remote_copy(
+            raw.at[k] if k < RAW else nb.at[k, pl.ds(0, count)],
+            rx.at[d - 1, k, pl.ds(0, count)],
+            sx_sem.at[d - 1, (k >= RAW) + (k >= LEAD)],
+            rx_sem.at[d - 1, k],
+            device_id=peer(d),
+            device_id_type=MESH,
+        )
+
+    def x_sent(d, first, stop, group, count=rows_each):
+        part = rx.at[d - 1, pl.ds(first, stop - first), pl.ds(0, count)]
+        return pltpu.make_async_remote_copy(
+            part, part, sx_sem.at[d - 1, group], rx_sem.at[d - 1, 0], device_id=peer(d), device_id_type=MESH
+        )
+
+    def x_arrival(d, k, count=rows_each):
+        part = rx.at[d - 1, k, pl.ds(0, count)]
+        return pltpu.make_async_remote_copy(
+            part, part, sx_sem.at[d - 1, 0], rx_sem.at[d - 1, k], device_id=peer(d), device_id_type=MESH
+        )
+
+    def by_block(act):
+        pl.when(lender)(lambda: act(kept))
+        pl.when(jnp.logical_not(lender))(lambda: act(rows_each))
+
+    def to_block(src, dst, send_sem, recv_sem, block, target):
+        return pltpu.make_async_remote_copy(
+            src, dst, send_sem, recv_sem, device_id={"sp": block, "tp": target}, device_id_type=MESH
+        )
+
+    lend = to_block(nb.at[:, pl.ds(kept, E)], lent, sl_sem, rl_sem, 0, tp)
+
+    def forward(d):
+        return pltpu.make_async_remote_copy(
+            lent, rx.at[d - 1, :, pl.ds(rows_each, E)], sf_sem.at[d - 1], rf_sem.at[d - 1],
+            device_id=peer(d), device_id_type=MESH,
+        )
+
+    def gate_copy(d, g):
+        return to_block(
+            gate_rep.at[d, S - 1, g, pl.ds(L - E, E)], gate_rep.at[d, S - 1, g, pl.ds(L, E)],
+            sg_sem.at[d - 1, g], rg_sem.at[d - 1, g], 0, tp,
+        )
+
+    def give_back(d, g):
+        return to_block(
+            lent_tx.at[d - 1, g], lent_rx.at[d - 1, g], sk_sem.at[d - 1, g], rk_sem.at[d - 1, g],
+            Z - 1, partner if g else tp,
         )
 
     def inv_copy(d):
@@ -120,15 +167,20 @@
         return (v.astype(f32) * r * gain_row[:, pl.ds(k * KC, KC)]).astype(bf)
 
     pltpu.make_async_copy(raw, raw, raw_sem).wait()
-    pl.semaphore_wait(barrier, 1 + (X - 1) + sides)
-
-    def send(chunks):
+    before = (z > 0).astype(jnp.int32)
+    pl.semaphore_wait(barrier, 1 + (X - 1) + before)
+
+    def send(chunks, count=rows_each):
         for k in chunks:
             for d in range(1, X):
-                x_copy(d, k).start()
-
-    pl.when(c == 0)(lambda: send(range(RAW)))
-    pl.when(c != 0)(lambda: send(range(RAW)))
+                x_copy(d, k, count).start()
+
+    send(range(RAW))
+
+    @pl.when(z > 0)
+    def _():
+        pl.semaphore_signal(answer_sem, inc=1, device_id={"sp": z - 1}, device_id_type=MESH)
+
 
     small[0].wait()
     g = gain_v[...].astype(f32)
@@ -149,23 +201,27 @@
     for k in range(RAW, NC):
         nb[k] = norm(tok[:, pl.ds(k * KC, KC)], inv[...], k)
         if k < LEAD:
-            send([k])
-        else:
-            pl.when(c == 0)(lambda k=k: send([k]))
+            by_block(lambda count: send([k], count))
         if k == RAW:
             for d in range(1, X):
                 inv_copy(d).start()
+        if k == HALF - 1:
+            pl.when(c == 0)(lambda: by_block(lambda count: send(range(LEAD, HALF), count)))
     for copy in shares[2:] + shares[:2]:
         copy.start()
     for k in range(RAW):
         nb[k] = norm(raw[k], inv[...], k)
-    if Z > 2:
-        greet_sides(hop_sem.at[0])
+    pl.when(z < Z - 1)(lambda: pl.semaphore_wait(answer_sem, 1))
+    for r in range(Z - 2):
+        greet_sides(hop_sem.at[r])
+        pl.semaphore_wait(hop_sem.at[r], sides)
+    pl.when(lender)(lend.start)
 
     @pl.when(c != 0)
     def _():
         for d in range(1, X):
-            x_whole(d, 0, LEAD, 0).wait_send()
+            x_sent(d, 0, RAW, 0).wait_send()
+            by_block(lambda count: x_sent(d, RAW, LEAD, 1, count).wait_send())
 
     small[1].wait()
     small[2].wait()
@@ -202,7 +258,12 @@
                 for h in range(H):
                     column = jnp.sum(jnp.where(pick, gates_v[g, s, h : h + 1, :], 0.0), axis=1, keepdims=True)
                     spread = jnp.where(head_of_lane == h, column, spread)
-                gate_rep[d, s, g] = spread
+                gate_rep[d, s, g, :L] = spread
+
+                @pl.when(jnp.logical_not(helper))
+                def _():
+                    gate_rep[d, s, g, L:] = jnp.full((E, C), -masked_score, f32)
+
     for s in range(S):
         fresh = jnp.dot(new_v[1, s : s + 1, :], qblock[s, 0], preferred_element_type=f32) * scale
         own_gate = jnp.sum(jnp.where(heads_eye, ng_v[s : s + 1, :], 0.0), axis=1, keepdims=True)
@@ -215,13 +276,16 @@
         stats_tx[1, 1, s : s + 1, :] = jnp.zeros((1, C), f32)
         stats_tx[1, 2, s : s + 1, :] = jnp.zeros((1, C), f32)
 
-    pl.when(c != 0)(lambda: send(range(LEAD, NC)))
+    pl.when(c != 0)(lambda: by_block(lambda count: send(range(LEAD, HALF), count)))
+    for d in range(1, X):
+        for g in range(CORES):
+            pl.when(lender)(gate_copy(d, g).start)
     for d in range(1, X):
         inv_copy(d).wait_recv()
         r = jnp.sum(jnp.where(eye, inv_rx[d - 1], 0.0), axis=1, keepdims=True)
-        x_whole(d, 0, RAW, 0).wait_recv()
         for k in range(RAW):
-            rx[d - 1, k] = norm(rx[d - 1, k], r, k)
+            x_arrival(d, k).wait_recv()
+            rx[d - 1, k, :rows_each] = norm(rx[d - 1, k, :rows_each], r, k)
 
     def w_part(k):
         return wbuf[pl.ds(k * KC if isinstance(k, int) else pl.multiple_of(k * KC, KC), KC), :]
@@ -232,18 +296,22 @@
             ybuf.at[d, v, pl.ds(s * L, L)], (kbuf, vbuf)[v].at[s, at],
             sy_sem, ry_sem, device_id={"tp": partner}, device_id_type=MESH,
         )
+
+    def rows_of(d, s):
+        return L + E if d and s == S - 1 else L
 
     def finish(d, y, last):
         pairs = [(g, s) for g in range(CORES) for s in range(S)]
         before = {(g, s): [stats_tx[g, i, s : s + 1, :] for i in range(3)] for g, s in pairs}
         scores = {}
         for g, s in pairs:
-            keys = y[s * L : (s + 1) * L, g * C : (g + 1) * C]
-            scores[g, s] = jnp.dot(keys, qblock[s, g], preferred_element_type=f32) * scale - gate_rep[d, s, g]
+            stop = rows_of(d, s)
+            keys = y[s * L : s * L + stop, g * C : (g + 1) * C]
+            scores[g, s] = jnp.dot(keys, qblock[s, g], preferred_element_type=f32) * scale - gate_rep[d, s, g, :stop]
         after = {}
         for g, s in pairs:
             old_top, old_total, old_weighted = before[g, s]
-            values = y[s * L : (s + 1) * L, (2 + g) * C : (3 + g) * C].astype(f32)
+            values = y[s * L : s * L + rows_of(d, s), (2 + g) * C : (3 + g) * C].astype(f32)
             top = jnp.maximum(jnp.max(scores[g, s], axis=0, keepdims=True), old_top)
             weights = jnp.exp(scores[g, s] - top)
             factor = jnp.exp(old_top - top)
@@ -264,8 +332,8 @@
             part = y[s * L : (s + 1) * L]
             kbuf[s, place, :] = part[:, :C]
             vbuf[s, place, :] = part[:, 2 * C : 3 * C]
-        ybuf[d, 0] = y[:, C : 2 * C]
-        ybuf[d, 1] = y[:, 3 * C :]
+        ybuf[d, 0] = y[:rows_each, C : 2 * C]
+        ybuf[d, 1] = y[:rows_each, 3 * C :]
 
     def send_partner(d):
         for s in range(S):
@@ -274,23 +342,35 @@
 
     pltpu.make_async_copy(wbuf.at[:, pl.ds(0, 2 * C)], wbuf.at[:, pl.ds(0, 2 * C)], w_sem).wait()
     both_weights.wait_recv()
+
+    @pl.when(helper)
+    def _():
+        to_block(lent, lent, sl_sem, rl_sem, 0, tp).wait_recv()
+        for d in range(1, X):
+            forward(d).start()
+
+    by_block(lambda count: send(range(HALF, NC), count))
     acc[...] = jnp.zeros_like(acc)
 
     def near(k, carry):
-        acc[...] += jnp.dot(nb[k], w_part(k), preferred_element_type=f32)
+        acc[:rows_each] += jnp.dot(nb[k], w_part(k), preferred_element_type=f32)
         return carry
 
     lax.fori_loop(0, NC, near, 0)
-    y = acc[...].astype(bf)
+    y = acc[:rows_each].astype(bf)
     deliver(0, y)
     finish(0, y, X == 1)
     send_partner(0)
-    for r in range(1, Z - 2):
-        pl.semaphore_wait(hop_sem.at[r - 1], sides)
-        greet_sides(hop_sem.at[r])
-    if Z > 2:
-        pl.semaphore_wait(hop_sem.at[Z - 3], sides)
     pl.semaphore_signal(ready_sem, inc=1, device_id={"tp": partner}, device_id_type=MESH)
+    for d in range(1, X):
+        for g in range(CORES):
+
+            @pl.when(lender)
+            def _(d=d, g=g):
+                gate_copy(d, g).wait_send()
+                gate_rep[d, S - 1, g, L - E : L] = jnp.full((E, C), -masked_score, f32)
+
+            pl.when(helper)(gate_copy(d, g).wait_recv)
     pl.semaphore_wait(ready_sem, 1)
 
     for d in range(1, X):
@@ -300,12 +380,23 @@
             acc[...] += jnp.dot(rx[d - 1, k], w_part(k), preferred_element_type=f32)
             return carry
 
-        for i, (start, stop) in enumerate(groups[:-1]):
-            if i:
-                x_whole(d, start, stop - start, i).wait_recv()
-            lax.fori_loop(start, stop, far, 0)
-        x_whole(d, NC - 1, 1, len(groups) - 1).wait_recv()
+        def far_arriving(k, carry, d=d):
+            by_block(lambda count: x_arrival(d, k, count).wait_recv())
+            return far(k, carry, d)
+
+        pl.when(helper)(forward(d).wait_recv)
+        lax.fori_loop(0, RAW, far, 0)
+        lax.fori_loop(RAW, NC - 1, far_arriving, 0)
+        by_block(lambda count: x_arrival(d, NC - 1, count).wait_recv())
         y = (acc[...] + jnp.dot(rx[d - 1, NC - 1], w_part(NC - 1), preferred_element_type=f32)).astype(bf)
+
+        @pl.when(helper)
+        def _(d=d, y=y):
+            for g in range(CORES):
+                for v in range(2):
+                    lent_tx[d - 1, g, v] = y[rows_each:, (2 * v + g) * C : (2 * v + g + 1) * C]
+                give_back(d, g).start()
+
         if d < X - 1:
             deliver(d, y)
             finish(d, y, False)
@@ -339,8 +430,17 @@
         send_partner(X - 1)
     for d in range(1, X):
         inv_copy(d).wait_send()
-        pl.when(c == 0)(x_whole(d, 0, NC, 0).wait_send)
-        pl.when(c != 0)(x_whole(d, LEAD, NC - LEAD, 0).wait_send)
+        pl.when(c == 0)(x_sent(d, 0, RAW, 0).wait_send)
+        pl.when(c == 0)(lambda: by_block(lambda count: x_sent(d, RAW, LEAD, 1, count).wait_send()))
+        by_block(lambda count: x_sent(d, LEAD, NC, 2, count).wait_send())
+
+        @pl.when(helper)
+        def _(d=d):
+            forward(d).wait_send()
+            for g in range(CORES):
+                give_back(d, g).wait_send()
+
+    pl.when(lender)(lend.wait_send)
     both_weights.wait_send()
     shares[2].wait_send()
     shares[3].wait_send()
@@ -358,6 +458,17 @@
     for other in range(CORES):
         if Z - 1 + other:
             z_whole(other).wait_recv()
+
+    @pl.when(lender)
+    def _():
+        for d in range(1, X):
+            for g in range(CORES):
+                give_back(d, g).wait_recv()
+                core = CORES - 1 - c if g else c
+                at = pl.ds(pl.multiple_of(((x + X - d) % X * CORES + core) * L + L - E, E), E)
+                kbuf[S - 1, at, :] = lent_rx[d - 1, g, 0]
+                vbuf[S - 1, at, :] = lent_rx[d - 1, g, 1]
+
     entries = [(i, other) for i in range(Z) for other in range(CORES)]
     tops = [stats_rx[other, i, 0] for i, other in entries]
     most = functools.reduce(jnp.maximum, tops)
@@ -368,6 +479,10 @@
     for other in range(CORES):
         if Z - 1 + other:
             z_whole(other).wait_send()
+
+
+def scoped(dims, semaphores, *refs):
+    pl.run_scoped(lambda *held: kernel(dims, *refs, *held), *semaphores)
 
 
 def write_out(*refs):
@@ -399,8 +514,15 @@
     regular = pltpu.SemaphoreType.REGULAR
     far = max(X - 1, 1)
     vmem = pl.BlockSpec(memory_space=pltpu.VMEM)
+    semaphores = [
+        dma((S * L // R,)), dma, dma, dma((4,)), regular((max(Z - 2, 1),)), regular, regular,
+        dma((far, 3)), dma((far, NC)), dma((far,)), dma((far,)), dma((3,)), dma((3,)),
+        dma, dma, dma((CORES,)), dma((CORES,)),
+        dma, dma, dma((far,)), dma((far,)),
+        dma((far, CORES)), dma((far, CORES)), dma((far, CORES)), dma((far, CORES)),
+    ]
     results = pl.pallas_call(
-        functools.partial(kernel, (S, L, R, T, Z)),
+        functools.partial(scoped, (S, L, R, T, Z), semaphores),
         out_shape=(
             pltpu.VMEM((S, BL, C), bf),
             pltpu.VMEM((S, BL, C), bf),
@@ -413,8 +535,8 @@
             pltpu.VMEM((RAW, S * L, KC), bf),
             pltpu.VMEM((S * L, KC), f32),
             pltpu.VMEM((NC, S * L, KC), bf),
-            pltpu.VMEM((far, NC, S * L, KC), bf),
-            pltpu.VMEM((S * L, 4 * C), f32),
+            pltpu.VMEM((far, NC, S * L + EXTRA, KC), bf),
+            pltpu.VMEM((S * L + EXTRA, 4 * C), f32),
             pltpu.VMEM((D, 4 * C), bf),
             pltpu.VMEM((X, 2, S * L, C), bf),
             pltpu.VMEM((D // 128, 128), bf),
@@ -425,12 +547,12 @@
             pltpu.VMEM((1, S * L), f32),
             pltpu.VMEM((far, 1, S * L), f32),
             pltpu.VMEM((S, CORES, C, C), bf),
-            pltpu.VMEM((X, S, CORES, L, C), f32),
+            pltpu.VMEM((X, S, CORES, L + EXTRA, C), f32),
             pltpu.VMEM((CORES, 3, S, C), f32),
             pltpu.VMEM((CORES, Z, 3, S, C), f32),
-            dma((S * L // R,)), dma, dma, dma((4,)), regular((max(Z - 2, 1),)), regular,
-            dma((far,)), dma((far, 5)), dma((far,)), dma((far,)), dma((3,)), dma((3,)),
-            dma, dma, dma((CORES,)), dma((CORES,)),
+            pltpu.VMEM((NC, EXTRA, KC), bf),
+            pltpu.VMEM((far, CORES, 2, EXTRA, C), bf),
+            pltpu.VMEM((far, CORES, 2, EXTRA, C), bf),
         ],
         compiler_params=pltpu.CompilerParams(
             collective_id=0, has_side_effects=True, vmem_limit_bytes=56 * 1024 * 1024

time: 34.3 us -> 32.9 us (0.959)
  Pallas kernels: 33.5 us -> 32.1 us
    pallas_call x1, Pallas kernels: 32.7 us -> 31.3 us  [body(): pl.pallas_call(functools.partial(scoped, (S, L, R, T, Z), semaphores), ou...]
where the time goes in v3:
time: 32.9 us; the launch traced here: 32.7 us
  Pallas kernels  32.1 us (98%)
  between operations  0.63 us (2%)
    pallas_call x1, Pallas kernels, body(): pl.pallas_call(functools.partial(scoped, (S, L, R, T, Z), semaphores), ou...  31.3 us
    pallas_call x1, Pallas kernels, body(): pl.pallas_call(write_out, out_shape=tuple((jax.ShapeDtypeStruct(r.shape,...  0.82 us

profile of v3, /device:TPU:0, one launch (start us, length us, event | category | flops | bytes accessed | tf_op | source)
XLA Modules:
  0.0 32.7 jit_solution(8988517960946995846)
XLA Ops:
  0.6 31.3 %shard_map.112 = (bf16[2,256,256]{2,1,0:T(8,128)(2,1)S(1)}, bf16[2,256,256]{2,1,0:T(8,128)(2,1)S(1)}, bf16[2,256]{1,0:T(2,128)(2,1)S(1)}) custom-call(bf16[128,4096]{1,0:T(8,128)(2,1)} %bitcast.3, bf16[32,128]{1,0:T(8,128)(2,1)} %bitcast.4, bf16[4096,256]{1,0:T(8,128)(2,1)} %refs_2_.1, bf16[4096,256]{1,0:T(8,128)(2,1)} %refs_3_.1, f32[2,4,256]{2,1,0:T(4,128)} %bitcast.5, ...), custom_call_target="tpu_custom_call" | custom-call | tf_op jit(solution)/shard_map/pallas_call | solution.py:524
  31.9 0.8 %shard_map.113 = (bf16[2,256,256]{2,1,0:T(8,128)(2,1)}, bf16[2,256,256]{2,1,0:T(8,128)(2,1)}, bf16[2,256]{1,0:T(2,128)(2,1)}) custom-call(bf16[2,256,256]{2,1,0:T(8,128)(2,1)S(1)} %get-tuple-element.6.refs_0_, bf16[2,256,256]{2,1,0:T(8,128)(2,1)S(1)} %get-tuple-element.7.refs_1_, bf16[2,256]{1,0:T(2,128)(2,1)S(1)} %get-tuple-element.8.refs_2_), custom_call_target="tpu_custom_call" | custom-call | tf_op jit(solution)/shard_map/pallas_call | solution.py:571

commit v4 on v3

--- a/solution.py
+++ b/solution.py
@@ -10,7 +10,8 @@
 HD = 64
 CORES = 2
 LEAD = 4
-EXTRA = 8
+TAIL = 4
+EXTRA, SLOTS = 8, 2
 RAW = 2
 
 epsilon = 1e-06
@@ -37,14 +38,21 @@
     C = kbuf.shape[2]
     H = C // HD
     BL = T * L
-    E = EXTRA
+    E, EE = EXTRA, SLOTS * EXTRA
     kept = rows_each - E
     tp = lax.axis_index("tp")
     z = lax.axis_index("sp")
     x, c = tp // CORES, tp % CORES
-    lender, helper = z == Z - 1, z == 0
-    if Z == 1:
-        lender = helper = z < 0
+    slots = [j for j in range(SLOTS) if Z - 1 - j > 0]
+
+    def lends(j, core):
+        return jnp.logical_and(z == Z - 1 - j, core >= j)
+
+    def helps(j, core):
+        return jnp.logical_and(z == 0, core >= j)
+
+    lender = functools.reduce(jnp.logical_or, [lends(j, c) for j in slots], z < 0)
+    pauses = c != 0
     partner = x * CORES + (CORES - 1 - c)
 
     def peer(d):
@@ -56,7 +64,7 @@
     first = [pltpu.make_async_copy(tok_hbm.at[:, pl.ds(k * KC, KC)], raw.at[k], raw_sem) for k in range(RAW)]
     for copy in first:
         copy.start()
-    rx[:, :, kept:, :] = jnp.zeros((rx.shape[0], NC, 2 * E, KC), bf)
+    rx[:, :, kept:, :] = jnp.zeros((rx.shape[0], NC, E + EE, KC), bf)
     barrier = pltpu.get_barrier_semaphore()
     for d in range(1, X):
         pl.semaphore_signal(barrier, inc=1, device_id=peer(d), device_id_type=MESH)
@@ -123,6 +131,15 @@
             part, part, sx_sem.at[d - 1, group], rx_sem.at[d - 1, 0], device_id=peer(d), device_id_type=MESH
         )
 
+    cut, split = (S - 1) * L, NC - TAIL
+
+    def x_part(d, k, part, count=rows_each):
+        at = pl.ds(cut, count - cut) if part else pl.ds(0, cut)
+        return pltpu.make_async_remote_copy(
+            nb.at[k, at], rx.at[d - 1, k, at], sx_sem.at[d - 1, 2], rx_sem.at[d - 1, k + TAIL * part],
+            device_id=peer(d), device_id_type=MESH,
+        )
+
     def x_arrival(d, k, count=rows_each):
         part = rx.at[d - 1, k, pl.ds(0, count)]
         return pltpu.make_async_remote_copy(
@@ -138,24 +155,25 @@
             src, dst, send_sem, recv_sem, device_id={"sp": block, "tp": target}, device_id_type=MESH
         )
 
-    lend = to_block(nb.at[:, pl.ds(kept, E)], lent, sl_sem, rl_sem, 0, tp)
-
-    def forward(d):
-        return pltpu.make_async_remote_copy(
-            lent, rx.at[d - 1, :, pl.ds(rows_each, E)], sf_sem.at[d - 1], rf_sem.at[d - 1],
+    def lend(j):
+        return to_block(nb.at[:, pl.ds(kept, E)], lent.at[j], sl_sem.at[j], rl_sem.at[j], 0, tp)
+
+    def forward(d, j):
+        return pltpu.make_async_remote_copy(
+            lent.at[j], rx.at[d - 1, :, pl.ds(rows_each + j * E, E)], sf_sem.at[d - 1, j], rf_sem.at[d - 1, j],
             device_id=peer(d), device_id_type=MESH,
         )
 
-    def gate_copy(d, g):
+    def gate_copy(d, g, j):
         return to_block(
-            gate_rep.at[d, S - 1, g, pl.ds(L - E, E)], gate_rep.at[d, S - 1, g, pl.ds(L, E)],
-            sg_sem.at[d - 1, g], rg_sem.at[d - 1, g], 0, tp,
-        )
-
-    def give_back(d, g):
+            gate_rep.at[d, S - 1, g, pl.ds(L - E, E)], gate_rep.at[d, S - 1, g, pl.ds(L + j * E, E)],
+            sg_sem.at[d - 1, g, j], rg_sem.at[d - 1, g, j], 0, tp,
+        )
+
+    def give_back(d, g, j):
         return to_block(
-            lent_tx.at[d - 1, g], lent_rx.at[d - 1, g], sk_sem.at[d - 1, g], rk_sem.at[d - 1, g],
-            Z - 1, partner if g else tp,
+            lent_tx.at[d - 1, g, j], lent_rx.at[d - 1, g], sk_sem.at[d - 1, g, j], rk_sem.at[d - 1, g, j],
+            Z - 1 - j, partner if g else tp,
         )
 
     def inv_copy(d):
@@ -206,7 +224,7 @@
             for d in range(1, X):
                 inv_copy(d).start()
         if k == HALF - 1:
-            pl.when(c == 0)(lambda: by_block(lambda count: send(range(LEAD, HALF), count)))
+            pl.when(jnp.logical_not(pauses))(lambda: by_block(lambda count: send(range(LEAD, HALF), count)))
     for copy in shares[2:] + shares[:2]:
         copy.start()
     for k in range(RAW):
@@ -215,9 +233,10 @@
     for r in range(Z - 2):
         greet_sides(hop_sem.at[r])
         pl.semaphore_wait(hop_sem.at[r], sides)
-    pl.when(lender)(lend.start)
-
-    @pl.when(c != 0)
+    for j in slots:
+        pl.when(lends(j, c))(lend(j).start)
+
+    @pl.when(pauses)
     def _():
         for d in range(1, X):
             x_sent(d, 0, RAW, 0).wait_send()
@@ -260,9 +279,12 @@
                     spread = jnp.where(head_of_lane == h, column, spread)
                 gate_rep[d, s, g, :L] = spread
 
-                @pl.when(jnp.logical_not(helper))
-                def _():
-                    gate_rep[d, s, g, L:] = jnp.full((E, C), -masked_score, f32)
+                for j in range(SLOTS):
+                    theirs = helps(j, c) if j in slots else z < 0
+
+                    @pl.when(jnp.logical_not(theirs))
+                    def _(d=d, s=s, g=g, j=j):
+                        gate_rep[d, s, g, L + j * E : L + (j + 1) * E] = jnp.full((E, C), -masked_score, f32)
 
     for s in range(S):
         fresh = jnp.dot(new_v[1, s : s + 1, :], qblock[s, 0], preferred_element_type=f32) * scale
@@ -276,10 +298,11 @@
         stats_tx[1, 1, s : s + 1, :] = jnp.zeros((1, C), f32)
         stats_tx[1, 2, s : s + 1, :] = jnp.zeros((1, C), f32)
 
-    pl.when(c != 0)(lambda: by_block(lambda count: send(range(LEAD, HALF), count)))
+    pl.when(pauses)(lambda: by_block(lambda count: send(range(LEAD, HALF), count)))
     for d in range(1, X):
         for g in range(CORES):
-            pl.when(lender)(gate_copy(d, g).start)
+            for j in slots:
+                pl.when(lends(j, c))(gate_copy(d, g, j).start)
     for d in range(1, X):
         inv_copy(d).wait_recv()
         r = jnp.sum(jnp.where(eye, inv_rx[d - 1], 0.0), axis=1, keepdims=True)
@@ -298,20 +321,20 @@
         )
 
     def rows_of(d, s):
-        return L + E if d and s == S - 1 else L
-
-    def finish(d, y, last):
-        pairs = [(g, s) for g in range(CORES) for s in range(S)]
+        return L + EE if d and s == S - 1 else L
+
+    def finish(d, y, first, prompts, last):
+        pairs = [(g, s) for g in range(CORES) for s in prompts]
         before = {(g, s): [stats_tx[g, i, s : s + 1, :] for i in range(3)] for g, s in pairs}
         scores = {}
         for g, s in pairs:
-            stop = rows_of(d, s)
-            keys = y[s * L : s * L + stop, g * C : (g + 1) * C]
-            scores[g, s] = jnp.dot(keys, qblock[s, g], preferred_element_type=f32) * scale - gate_rep[d, s, g, :stop]
+            count = rows_of(d, s)
+            keys = y[s * L - first : s * L - first + count, g * C : (g + 1) * C]
+            scores[g, s] = jnp.dot(keys, qblock[s, g], preferred_element_type=f32) * scale - gate_rep[d, s, g, :count]
         after = {}
         for g, s in pairs:
             old_top, old_total, old_weighted = before[g, s]
-            values = y[s * L : s * L + rows_of(d, s), (2 + g) * C : (3 + g) * C].astype(f32)
+            values = y[s * L - first : s * L - first + rows_of(d, s), (2 + g) * C : (3 + g) * C].astype(f32)
             top = jnp.maximum(jnp.max(scores[g, s], axis=0, keepdims=True), old_top)
             weights = jnp.exp(scores[g, s] - top)
             factor = jnp.exp(old_top - top)
@@ -322,34 +345,40 @@
             for i, row in enumerate(after[g, s]):
                 stats_tx[g, i, s : s + 1, :] = row
         if last:
-            for s in range(S):
+            for s in prompts:
                 for i, row in enumerate(after[0, s]):
                     stats_rx[0, z, i, s : s + 1, :] = row
 
-    def deliver(d, y):
+    def deliver(d, y, first, prompts):
         place = pl.ds(pl.multiple_of(source(d) * L, L), L)
-        for s in range(S):
-            part = y[s * L : (s + 1) * L]
+        for s in prompts:
+            part = y[s * L - first : (s + 1) * L - first]
             kbuf[s, place, :] = part[:, :C]
             vbuf[s, place, :] = part[:, 2 * C : 3 * C]
-        ybuf[d, 0] = y[:rows_each, C : 2 * C]
-        ybuf[d, 1] = y[:rows_each, 3 * C :]
-
-    def send_partner(d):
-        for s in range(S):
+            ybuf[d, 0, s * L : (s + 1) * L] = part[:, C : 2 * C]
+            ybuf[d, 1, s * L : (s + 1) * L] = part[:, 3 * C :]
+
+    def send_partner(d, prompts):
+        for s in prompts:
             for v in range(2):
                 y_copy(d, s, v).start()
 
     pltpu.make_async_copy(wbuf.at[:, pl.ds(0, 2 * C)], wbuf.at[:, pl.ds(0, 2 * C)], w_sem).wait()
     both_weights.wait_recv()
 
-    @pl.when(helper)
-    def _():
-        to_block(lent, lent, sl_sem, rl_sem, 0, tp).wait_recv()
-        for d in range(1, X):
-            forward(d).start()
-
-    by_block(lambda count: send(range(HALF, NC), count))
+    for j in slots:
+
+        @pl.when(helps(j, c))
+        def _(j=j):
+            lend(j).wait_recv()
+            for d in range(1, X):
+                forward(d, j).start()
+
+    by_block(lambda count: send(range(HALF, split), count))
+    for part in range(2):
+        for k in range(split, NC):
+            for d in range(1, X):
+                by_block(lambda count: x_part(d, k, part, count).start())
     acc[...] = jnp.zeros_like(acc)
 
     def near(k, carry):
@@ -358,19 +387,21 @@
 
     lax.fori_loop(0, NC, near, 0)
     y = acc[:rows_each].astype(bf)
-    deliver(0, y)
-    finish(0, y, X == 1)
-    send_partner(0)
+    deliver(0, y, 0, range(S))
+    finish(0, y, 0, range(S), X == 1)
+    send_partner(0, range(S))
     pl.semaphore_signal(ready_sem, inc=1, device_id={"tp": partner}, device_id_type=MESH)
     for d in range(1, X):
         for g in range(CORES):
 
-            @pl.when(lender)
-            def _(d=d, g=g):
-                gate_copy(d, g).wait_send()
-                gate_rep[d, S - 1, g, L - E : L] = jnp.full((E, C), -masked_score, f32)
-
-            pl.when(helper)(gate_copy(d, g).wait_recv)
+            for j in slots:
+
+                @pl.when(lends(j, c))
+                def _(d=d, g=g, j=j):
+                    gate_copy(d, g, j).wait_send()
+                    gate_rep[d, S - 1, g, L - E : L] = jnp.full((E, C), -masked_score, f32)
+
+                pl.when(helps(j, c))(gate_copy(d, g, j).wait_recv)
     pl.semaphore_wait(ready_sem, 1)
 
     for d in range(1, X):
@@ -384,25 +415,39 @@
             by_block(lambda count: x_arrival(d, k, count).wait_recv())
             return far(k, carry, d)
 
-        pl.when(helper)(forward(d).wait_recv)
+        for j in slots:
+            pl.when(helps(j, c))(forward(d, j).wait_recv)
         lax.fori_loop(0, RAW, far, 0)
-        lax.fori_loop(RAW, NC - 1, far_arriving, 0)
-        by_block(lambda count: x_arrival(d, NC - 1, count).wait_recv())
-        y = (acc[...] + jnp.dot(rx[d - 1, NC - 1], w_part(NC - 1), preferred_element_type=f32)).astype(bf)
-
-        @pl.when(helper)
-        def _(d=d, y=y):
-            for g in range(CORES):
-                for v in range(2):
-                    lent_tx[d - 1, g, v] = y[rows_each:, (2 * v + g) * C : (2 * v + g + 1) * C]
-                give_back(d, g).start()
-
-        if d < X - 1:
-            deliver(d, y)
-            finish(d, y, False)
-            send_partner(d)
-        else:
-            finish(d, y, True)
+        lax.fori_loop(RAW, split, far_arriving, 0)
+        last = d == X - 1
+        if cut:
+            for k in range(split, NC):
+                x_part(d, k, 0).wait_recv()
+                acc[:cut] += jnp.dot(rx[d - 1, k, :cut], w_part(k), preferred_element_type=f32)
+            y = acc[:cut].astype(bf)
+            finish(d, y, 0, range(S - 1), last)
+            fronts = y
+        for k in range(split, NC - 1):
+            by_block(lambda count: x_part(d, k, 1, count).wait_recv())
+            acc[cut:] += jnp.dot(rx[d - 1, k, cut:], w_part(k), preferred_element_type=f32)
+        by_block(lambda count: x_part(d, NC - 1, 1, count).wait_recv())
+        y = (acc[cut:] + jnp.dot(rx[d - 1, NC - 1, cut:], w_part(NC - 1), preferred_element_type=f32)).astype(bf)
+
+        for j in slots:
+
+            @pl.when(helps(j, c))
+            def _(d=d, y=y, j=j):
+                for g in range(CORES):
+                    for v in range(2):
+                        lent_tx[d - 1, g, j, v] = y[L + j * E : L + (j + 1) * E, (2 * v + g) * C : (2 * v + g + 1) * C]
+                    give_back(d, g, j).start()
+
+        finish(d, y, cut, [S - 1], last)
+        if not last:
+            if cut:
+                deliver(d, fronts, 0, range(S - 1))
+            deliver(d, y, cut, [S - 1])
+            send_partner(d, range(S))
 
     def z_target(i):
         return jnp.where(2 * z >= Z, i, Z - 1 - i)
@@ -426,21 +471,26 @@
                         z_copy(i, 1).start()
 
     if X > 1:
-        deliver(X - 1, y)
-        send_partner(X - 1)
+        if cut:
+            deliver(X - 1, fronts, 0, range(S - 1))
+        deliver(X - 1, y, cut, [S - 1])
+        send_partner(X - 1, range(S))
     for d in range(1, X):
         inv_copy(d).wait_send()
-        pl.when(c == 0)(x_sent(d, 0, RAW, 0).wait_send)
-        pl.when(c == 0)(lambda: by_block(lambda count: x_sent(d, RAW, LEAD, 1, count).wait_send()))
+        pl.when(jnp.logical_not(pauses))(x_sent(d, 0, RAW, 0).wait_send)
+        pl.when(jnp.logical_not(pauses))(lambda: by_block(lambda count: x_sent(d, RAW, LEAD, 1, count).wait_send()))
         by_block(lambda count: x_sent(d, LEAD, NC, 2, count).wait_send())
 
-        @pl.when(helper)
-        def _(d=d):
-            forward(d).wait_send()
-            for g in range(CORES):
-                give_back(d, g).wait_send()
-
-    pl.when(lender)(lend.wait_send)
+        for j in slots:
+
+            @pl.when(helps(j, c))
+            def _(d=d, j=j):
+                forward(d, j).wait_send()
+                for g in range(CORES):
+                    give_back(d, g, j).wait_send()
+
+    for j in slots:
+        pl.when(lends(j, c))(lend(j).wait_send)
     both_weights.wait_send()
     shares[2].wait_send()
     shares[3].wait_send()
@@ -459,15 +509,17 @@
         if Z - 1 + other:
             z_whole(other).wait_recv()
 
-    @pl.when(lender)
-    def _():
-        for d in range(1, X):
-            for g in range(CORES):
-                give_back(d, g).wait_recv()
-                core = CORES - 1 - c if g else c
-                at = pl.ds(pl.multiple_of(((x + X - d) % X * CORES + core) * L + L - E, E), E)
-                kbuf[S - 1, at, :] = lent_rx[d - 1, g, 0]
-                vbuf[S - 1, at, :] = lent_rx[d - 1, g, 1]
+    for j in slots:
+        for g in range(CORES):
+            core = CORES - 1 - c if g else c
+
+            @pl.when(lends(j, core))
+            def _(g=g, j=j, core=core):
+                for d in range(1, X):
+                    give_back(d, g, j).wait_recv()
+                    at = pl.ds(pl.multiple_of(((x + X - d) % X * CORES + core) * L + L - E, E), E)
+                    kbuf[S - 1, at, :] = lent_rx[d - 1, g, 0]
+                    vbuf[S - 1, at, :] = lent_rx[d - 1, g, 1]
 
     entries = [(i, other) for i in range(Z) for other in range(CORES)]
     tops = [stats_rx[other, i, 0] for i, other in entries]
@@ -516,10 +568,10 @@
     vmem = pl.BlockSpec(memory_space=pltpu.VMEM)
     semaphores = [
         dma((S * L // R,)), dma, dma, dma((4,)), regular((max(Z - 2, 1),)), regular, regular,
-        dma((far, 3)), dma((far, NC)), dma((far,)), dma((far,)), dma((3,)), dma((3,)),
+        dma((far, 3)), dma((far, NC + TAIL)), dma((far,)), dma((far,)), dma((3,)), dma((3,)),
         dma, dma, dma((CORES,)), dma((CORES,)),
-        dma, dma, dma((far,)), dma((far,)),
-        dma((far, CORES)), dma((far, CORES)), dma((far, CORES)), dma((far, CORES)),
+        dma((SLOTS,)), dma((SLOTS,)), dma((far, SLOTS)), dma((far, SLOTS)),
+        *(dma((far, CORES, SLOTS)) for _ in range(4)),
     ]
     results = pl.pallas_call(
         functools.partial(scoped, (S, L, R, T, Z), semaphores),
@@ -535,8 +587,8 @@
             pltpu.VMEM((RAW, S * L, KC), bf),
             pltpu.VMEM((S * L, KC), f32),
             pltpu.VMEM((NC, S * L, KC), bf),
-            pltpu.VMEM((far, NC, S * L + EXTRA, KC), bf),
-            pltpu.VMEM((S * L + EXTRA, 4 * C), f32),
+            pltpu.VMEM((far, NC, S * L + SLOTS * EXTRA, KC), bf),
+            pltpu.VMEM((S * L + SLOTS * EXTRA, 4 * C), f32),
             pltpu.VMEM((D, 4 * C), bf),
             pltpu.VMEM((X, 2, S * L, C), bf),
             pltpu.VMEM((D // 128, 128), bf),
@@ -547,11 +599,11 @@
             pltpu.VMEM((1, S * L), f32),
             pltpu.VMEM((far, 1, S * L), f32),
             pltpu.VMEM((S, CORES, C, C), bf),
-            pltpu.VMEM((X, S, CORES, L + EXTRA, C), f32),
+            pltpu.VMEM((X, S, CORES, L + SLOTS * EXTRA, C), f32),
             pltpu.VMEM((CORES, 3, S, C), f32),
             pltpu.VMEM((CORES, Z, 3, S, C), f32),
-            pltpu.VMEM((NC, EXTRA, KC), bf),
-            pltpu.VMEM((far, CORES, 2, EXTRA, C), bf),
+            pltpu.VMEM((SLOTS, NC, EXTRA, KC), bf),
+            pltpu.VMEM((far, CORES, SLOTS, 2, EXTRA, C), bf),
             pltpu.VMEM((far, CORES, 2, EXTRA, C), bf),
         ],
         compiler_params=pltpu.CompilerParams(

time: 32.9 us -> 32.8 us (level)
  no operation moved by 1% of the time
where the time goes in v4:
time: 32.8 us; the launch traced here: 32.7 us
  Pallas kernels  32 us (98%)
  between operations  0.63 us (2%)
    pallas_call x1, Pallas kernels, body(): pl.pallas_call(functools.partial(scoped, (S, L, R, T, Z), semaphores), ou...  31.2 us
    pallas_call x1, Pallas kernels, body(): pl.pallas_call(write_out, out_shape=tuple((jax.ShapeDtypeStruct(r.shape,...  0.82 us

profile of v4, /device:TPU:0, one launch (start us, length us, event | category | flops | bytes accessed | tf_op | source)
XLA Modules:
  0.0 32.7 jit_solution(15064048599917165867)
XLA Ops:
  0.6 31.2 %shard_map.112 = (bf16[2,256,256]{2,1,0:T(8,128)(2,1)S(1)}, bf16[2,256,256]{2,1,0:T(8,128)(2,1)S(1)}, bf16[2,256]{1,0:T(2,128)(2,1)S(1)}) custom-call(bf16[128,4096]{1,0:T(8,128)(2,1)} %bitcast.3, bf16[32,128]{1,0:T(8,128)(2,1)} %bitcast.4, bf16[4096,256]{1,0:T(8,128)(2,1)} %refs_2_.1, bf16[4096,256]{1,0:T(8,128)(2,1)} %refs_3_.1, f32[2,4,256]{2,1,0:T(4,128)} %bitcast.5, ...), custom_call_target="tpu_custom_call" | custom-call | tf_op jit(solution)/shard_map/pallas_call | solution.py:576
  31.8 0.8 %shard_map.113 = (bf16[2,256,256]{2,1,0:T(8,128)(2,1)}, bf16[2,256,256]{2,1,0:T(8,128)(2,1)}, bf16[2,256]{1,0:T(2,128)(2,1)}) custom-call(bf16[2,256,256]{2,1,0:T(8,128)(2,1)S(1)} %get-tuple-element.6.refs_0_, bf16[2,256,256]{2,1,0:T(8,128)(2,1)S(1)} %get-tuple-element.7.refs_1_, bf16[2,256]{1,0:T(2,128)(2,1)S(1)} %get-tuple-element.8.refs_2_), custom_call_target="tpu_custom_call" | custom-call | tf_op jit(solution)/shard_map/pallas_call | solution.py:623

commit v5 on v4

--- a/solution.py
+++ b/solution.py
@@ -39,19 +39,20 @@
     H = C // HD
     BL = T * L
     E, EE = EXTRA, SLOTS * EXTRA
-    kept = rows_each - E
+    kept = rows_each - 2 * E
     tp = lax.axis_index("tp")
     z = lax.axis_index("sp")
     x, c = tp // CORES, tp % CORES
-    slots = [j for j in range(SLOTS) if Z - 1 - j > 0]
+    loans = [(Z - 1, 0, 0, 0, E), (Z - 2, 0, 1, 1, E), (Z - 1, 1, 1, 1, 2 * E)][: 3 if Z > 3 else min(Z - 1, 2)]
+    slots = range(len(loans))
 
     def lends(j, core):
-        return jnp.logical_and(z == Z - 1 - j, core >= j)
+        return jnp.logical_and(z == loans[j][0], core >= loans[j][2])
 
     def helps(j, core):
-        return jnp.logical_and(z == 0, core >= j)
-
-    lender = functools.reduce(jnp.logical_or, [lends(j, c) for j in slots], z < 0)
+        return jnp.logical_and(z == loans[j][1], core >= loans[j][2])
+
+    lent_rows = sum((lends(j, c).astype(jnp.int32) for j in slots), 0 * z)
     pauses = c != 0
     partner = x * CORES + (CORES - 1 - c)
 
@@ -61,10 +62,10 @@
     def rows(j):
         return pl.ds(j * R, R)
 
-    first = [pltpu.make_async_copy(tok_hbm.at[:, pl.ds(k * KC, KC)], raw.at[k], raw_sem) for k in range(RAW)]
+    first = [pltpu.make_async_copy(tok_hbm.at[:, pl.ds(k * KC, KC)], raw.at[k], raw_sem.at[k]) for k in range(RAW)]
     for copy in first:
         copy.start()
-    rx[:, :, kept:, :] = jnp.zeros((rx.shape[0], NC, E + EE, KC), bf)
+    rx[:, :, kept:, :] = jnp.zeros((rx.shape[0], NC, 2 * E + EE, KC), bf)
     barrier = pltpu.get_barrier_semaphore()
     for d in range(1, X):
         pl.semaphore_signal(barrier, inc=1, device_id=peer(d), device_id_type=MESH)
@@ -147,8 +148,8 @@
         )
 
     def by_block(act):
-        pl.when(lender)(lambda: act(kept))
-        pl.when(jnp.logical_not(lender))(lambda: act(rows_each))
+        for i in range(3):
+            pl.when(lent_rows == i)(lambda: act(rows_each - i * E))
 
     def to_block(src, dst, send_sem, recv_sem, block, target):
         return pltpu.make_async_remote_copy(
@@ -156,24 +157,27 @@
         )
 
     def lend(j):
-        return to_block(nb.at[:, pl.ds(kept, E)], lent.at[j], sl_sem.at[j], rl_sem.at[j], 0, tp)
+        _, block, _, slot, back = loans[j]
+        return to_block(nb.at[:, pl.ds(rows_each - back, E)], lent.at[slot], sl_sem.at[j], rl_sem.at[j], block, tp)
 
     def forward(d, j):
-        return pltpu.make_async_remote_copy(
-            lent.at[j], rx.at[d - 1, :, pl.ds(rows_each + j * E, E)], sf_sem.at[d - 1, j], rf_sem.at[d - 1, j],
+        slot = loans[j][3]
+        return pltpu.make_async_remote_copy(
+            lent.at[slot], rx.at[d - 1, :, pl.ds(rows_each + slot * E, E)], sf_sem.at[d - 1, j], rf_sem.at[d - 1, j],
             device_id=peer(d), device_id_type=MESH,
         )
 
     def gate_copy(d, g, j):
+        _, block, _, slot, back = loans[j]
         return to_block(
-            gate_rep.at[d, S - 1, g, pl.ds(L - E, E)], gate_rep.at[d, S - 1, g, pl.ds(L + j * E, E)],
-            sg_sem.at[d - 1, g, j], rg_sem.at[d - 1, g, j], 0, tp,
+            gate_rep.at[d, S - 1, g, pl.ds(L - back, E)], gate_rep.at[d, S - 1, g, pl.ds(L + slot * E, E)],
+            sg_sem.at[d - 1, g, j], rg_sem.at[d - 1, g, j], block, tp,
         )
 
     def give_back(d, g, j):
         return to_block(
-            lent_tx.at[d - 1, g, j], lent_rx.at[d - 1, g], sk_sem.at[d - 1, g, j], rk_sem.at[d - 1, g, j],
-            Z - 1 - j, partner if g else tp,
+            lent_tx.at[d - 1, g, loans[j][3]], lent_rx.at[d - 1, g, j], sk_sem.at[d - 1, g, j], rk_sem.at[d - 1, g, j],
+            loans[j][0], partner if g else tp,
         )
 
     def inv_copy(d):
@@ -184,7 +188,6 @@
     def norm(v, r, k):
         return (v.astype(f32) * r * gain_row[:, pl.ds(k * KC, KC)]).astype(bf)
 
-    pltpu.make_async_copy(raw, raw, raw_sem).wait()
     before = (z > 0).astype(jnp.int32)
     pl.semaphore_wait(barrier, 1 + (X - 1) + before)
 
@@ -193,7 +196,9 @@
             for d in range(1, X):
                 x_copy(d, k, count).start()
 
-    send(range(RAW))
+    for k in range(RAW):
+        first[k].wait()
+        send([k])
 
     @pl.when(z > 0)
     def _():
@@ -279,12 +284,12 @@
                     spread = jnp.where(head_of_lane == h, column, spread)
                 gate_rep[d, s, g, :L] = spread
 
-                for j in range(SLOTS):
-                    theirs = helps(j, c) if j in slots else z < 0
+                for slot in range(SLOTS):
+                    theirs = functools.reduce(jnp.logical_or, [helps(j, c) for j in slots if loans[j][3] == slot], z < 0)
 
                     @pl.when(jnp.logical_not(theirs))
-                    def _(d=d, s=s, g=g, j=j):
-                        gate_rep[d, s, g, L + j * E : L + (j + 1) * E] = jnp.full((E, C), -masked_score, f32)
+                    def _(d=d, s=s, g=g, slot=slot):
+                        gate_rep[d, s, g, L + slot * E : L + (slot + 1) * E] = jnp.full((E, C), -masked_score, f32)
 
     for s in range(S):
         fresh = jnp.dot(new_v[1, s : s + 1, :], qblock[s, 0], preferred_element_type=f32) * scale
@@ -399,7 +404,8 @@
                 @pl.when(lends(j, c))
                 def _(d=d, g=g, j=j):
                     gate_copy(d, g, j).wait_send()
-                    gate_rep[d, S - 1, g, L - E : L] = jnp.full((E, C), -masked_score, f32)
+                    back = L - loans[j][4]
+                    gate_rep[d, S - 1, g, back : back + E] = jnp.full((E, C), -masked_score, f32)
 
                 pl.when(helps(j, c))(gate_copy(d, g, j).wait_recv)
     pl.semaphore_wait(ready_sem, 1)
@@ -439,7 +445,9 @@
             def _(d=d, y=y, j=j):
                 for g in range(CORES):
                     for v in range(2):
-                        lent_tx[d - 1, g, j, v] = y[L + j * E : L + (j + 1) * E, (2 * v + g) * C : (2 * v + g + 1) * C]
+                        slot = loans[j][3]
+                        rows_back = y[L + slot * E : L + (slot + 1) * E]
+                        lent_tx[d - 1, g, slot, v] = rows_back[:, (2 * v + g) * C : (2 * v + g + 1) * C]
                     give_back(d, g, j).start()
 
         finish(d, y, cut, [S - 1], last)
@@ -517,9 +525,9 @@
             def _(g=g, j=j, core=core):
                 for d in range(1, X):
                     give_back(d, g, j).wait_recv()
-                    at = pl.ds(pl.multiple_of(((x + X - d) % X * CORES + core) * L + L - E, E), E)
-                    kbuf[S - 1, at, :] = lent_rx[d - 1, g, 0]
-                    vbuf[S - 1, at, :] = lent_rx[d - 1, g, 1]
+                    at = pl.ds(pl.multiple_of(((x + X - d) % X * CORES + core) * L + L - loans[j][4], E), E)
+                    kbuf[S - 1, at, :] = lent_rx[d - 1, g, j, 0]
+                    vbuf[S - 1, at, :] = lent_rx[d - 1, g, j, 1]
 
     entries = [(i, other) for i in range(Z) for other in range(CORES)]
     tops = [stats_rx[other, i, 0] for i, other in entries]
@@ -567,11 +575,11 @@
     far = max(X - 1, 1)
     vmem = pl.BlockSpec(memory_space=pltpu.VMEM)
     semaphores = [
-        dma((S * L // R,)), dma, dma, dma((4,)), regular((max(Z - 2, 1),)), regular, regular,
+        dma((S * L // R,)), dma((RAW,)), dma, dma((4,)), regular((max(Z - 2, 1),)), regular, regular,
         dma((far, 3)), dma((far, NC + TAIL)), dma((far,)), dma((far,)), dma((3,)), dma((3,)),
         dma, dma, dma((CORES,)), dma((CORES,)),
-        dma((SLOTS,)), dma((SLOTS,)), dma((far, SLOTS)), dma((far, SLOTS)),
-        *(dma((far, CORES, SLOTS)) for _ in range(4)),
+        dma((3,)), dma((3,)), dma((far, 3)), dma((far, 3)),
+        *(dma((far, CORES, 3)) for _ in range(4)),
     ]
     results = pl.pallas_call(
         functools.partial(scoped, (S, L, R, T, Z), semaphores),
@@ -604,7 +612,7 @@
             pltpu.VMEM((CORES, Z, 3, S, C), f32),
             pltpu.VMEM((SLOTS, NC, EXTRA, KC), bf),
             pltpu.VMEM((far, CORES, SLOTS, 2, EXTRA, C), bf),
-            pltpu.VMEM((far, CORES, 2, EXTRA, C), bf),
+            pltpu.VMEM((far, CORES, 3, 2, EXTRA, C), bf),
         ],
         compiler_params=pltpu.CompilerParams(
             collective_id=0, has_side_effects=True, vmem_limit_bytes=56 * 1024 * 1024

time: 32.8 us -> 32.5 us (level)
  no operation moved by 1% of the time
where the time goes in v5:
time: 32.5 us; the launch traced here: 32.3 us
  Pallas kernels  31.7 us (98%)
  between operations  0.63 us (2%)
    pallas_call x1, Pallas kernels, body(): pl.pallas_call(functools.partial(scoped, (S, L, R, T, Z), semaphores), ou...  30.9 us
    pallas_call x1, Pallas kernels, body(): pl.pallas_call(write_out, out_shape=tuple((jax.ShapeDtypeStruct(r.shape,...  0.82 us

profile of v5, /device:TPU:0, one launch (start us, length us, event | category | flops | bytes accessed | tf_op | source)
XLA Modules:
  0.0 32.3 jit_solution(12699017577992375492)
XLA Ops:
  0.6 30.9 %shard_map.112 = (bf16[2,256,256]{2,1,0:T(8,128)(2,1)S(1)}, bf16[2,256,256]{2,1,0:T(8,128)(2,1)S(1)}, bf16[2,256]{1,0:T(2,128)(2,1)S(1)}) custom-call(bf16[128,4096]{1,0:T(8,128)(2,1)} %bitcast.3, bf16[32,128]{1,0:T(8,128)(2,1)} %bitcast.4, bf16[4096,256]{1,0:T(8,128)(2,1)} %refs_2_.1, bf16[4096,256]{1,0:T(8,128)(2,1)} %refs_3_.1, f32[2,4,256]{2,1,0:T(4,128)} %bitcast.5, ...), custom_call_target="tpu_custom_call" | custom-call | tf_op jit(solution)/shard_map/pallas_call | solution.py:584
  31.5 0.8 %shard_map.113 = (bf16[2,256,256]{2,1,0:T(8,128)(2,1)}, bf16[2,256,256]{2,1,0:T(8,128)(2,1)}, bf16[2,256]{1,0:T(2,128)(2,1)}) custom-call(bf16[2,256,256]{2,1,0:T(8,128)(2,1)S(1)} %get-tuple-element.6.refs_0_, bf16[2,256,256]{2,1,0:T(8,128)(2,1)S(1)} %get-tuple-element.7.refs_1_, bf16[2,256]{1,0:T(2,128)(2,1)S(1)} %get-tuple-element.8.refs_2_), custom_call_target="tpu_custom_call" | custom-call | tf_op jit(solution)/shard_map/pallas_call | solution.py:631

commit v6 on v5

--- a/solution.py
+++ b/solution.py
@@ -9,7 +9,7 @@
 
 HD = 64
 CORES = 2
-LEAD = 4
+LEAD = 3
 TAIL = 4
 EXTRA, SLOTS = 8, 2
 RAW = 2
@@ -546,13 +546,16 @@
 
 
 def write_out(*refs):
-    sems = refs[-1]
-    count = (len(refs) - 1) // 2
-    copies = [pltpu.make_async_copy(refs[i], refs[count + i], sems.at[i]) for i in range(count)]
-    for copy in copies:
-        copy.start()
-    for copy in copies:
-        copy.wait()
+    count = len(refs) // 2
+
+    def move(sems):
+        copies = [pltpu.make_async_copy(refs[i], refs[count + i], sems.at[i]) for i in range(count)]
+        for copy in copies:
+            copy.start()
+        for copy in copies:
+            copy.wait()
+
+    pl.run_scoped(move, pltpu.SemaphoreType.DMA((count,)))
 
 
 def body(
@@ -633,7 +636,6 @@
         out_shape=tuple(jax.ShapeDtypeStruct(r.shape, r.dtype) for r in results),
         in_specs=[vmem] * 3,
         out_specs=(hbm, hbm, hbm),
-        scratch_shapes=[dma((3,))],
     )(*(pltpu.with_memory_space_constraint(r, pltpu.VMEM) for r in results))
 
 

time: 32.5 us -> 32.5 us (level)
  no operation moved by 1% of the time
where the time goes in v6:
time: 32.5 us; the launch traced here: 32.3 us
  Pallas kernels  31.7 us (98%)
  between operations  0.63 us (2%)
    pallas_call x1, Pallas kernels, body(): pl.pallas_call(functools.partial(scoped, (S, L, R, T, Z), semaphores), ou...  30.9 us
    pallas_call x1, Pallas kernels, body(): pl.pallas_call(write_out, out_shape=tuple((jax.ShapeDtypeStruct(r.shape,...  0.8 us

profile of v6, /device:TPU:0, one launch (start us, length us, event | category | flops | bytes accessed | tf_op | source)
XLA Modules:
  0.0 32.3 jit_solution(4409041687735056662)
XLA Ops:
  0.6 30.9 %shard_map.112 = (bf16[2,256,256]{2,1,0:T(8,128)(2,1)S(1)}, bf16[2,256,256]{2,1,0:T(8,128)(2,1)S(1)}, bf16[2,256]{1,0:T(2,128)(2,1)S(1)}) custom-call(bf16[128,4096]{1,0:T(8,128)(2,1)} %bitcast.3, bf16[32,128]{1,0:T(8,128)(2,1)} %bitcast.4, bf16[4096,256]{1,0:T(8,128)(2,1)} %refs_2_.1, bf16[4096,256]{1,0:T(8,128)(2,1)} %refs_3_.1, f32[2,4,256]{2,1,0:T(4,128)} %bitcast.5, ...), custom_call_target="tpu_custom_call" | custom-call | tf_op jit(solution)/shard_map/pallas_call | solution.py:587
  31.5 0.8 %shard_map.113 = (bf16[2,256,256]{2,1,0:T(8,128)(2,1)}, bf16[2,256,256]{2,1,0:T(8,128)(2,1)}, bf16[2,256]{1,0:T(2,128)(2,1)}) custom-call(bf16[2,256,256]{2,1,0:T(8,128)(2,1)S(1)} %get-tuple-element.6.refs_0_, bf16[2,256,256]{2,1,0:T(8,128)(2,1)S(1)} %get-tuple-element.7.refs_1_, bf16[2,256]{1,0:T(2,128)(2,1)S(1)} %get-tuple-element.8.refs_2_), custom_call_target="tpu_custom_call" | custom-call | tf_op jit(solution)/shard_map/pallas_call | solution.py:634
